TPU v7x, 512 devices: a whole 4x4x16 slice. The times are simulated.
512 devices in a mesh: sp: 64 (over z, y), tp: 8 (over x, core).
Axes of the slice: x: 4, y: 4, z: 16, core: 2. Of those that a mesh axis runs over, the one named last changes fastest.
Arguments:
- latent: bfloat16 [49152, 2048], P(('sp', 'tp')), may hold values from -6 to 6
- condition: float32 [2048], P('sp'), may hold values from -6 to 6
- context_condition: float32 [2048], P('sp'), may hold values from -6 to 6
- context: bfloat16 [1024, 2048], P('sp'), may hold values from -6 to 6
- norm_gain: float32 [2048], replicated, may hold values from 0.1 to 1.9
- shift_weight: bfloat16 [2048, 2048], P('sp', 'tp'), may hold values from -0.375 to 0.375
- scale_weight: bfloat16 [2048, 2048], P('sp', 'tp'), may hold values from -0.375 to 0.375
- gate_weight: bfloat16 [2048, 2048], P('sp', 'tp'), may hold values from -0.375 to 0.375
- query_weight: bfloat16 [2048, 2048], P(None, 'tp'), may hold values from -2 to 2
- key_matrix: bfloat16 [2048, 1024], P(None, 'tp'), may hold values from -2 to 2
- value_matrix: bfloat16 [2048, 1024], P(None, 'tp'), may hold values from -0.125 to 0.125
- sink_logit_head: float32 [16], P('tp'), may hold values from 6 to 10
- out_weight: bfloat16 [2048, 2048], P('tp'), may hold values from -0.125 to 0.125
Outputs:
- updated: bfloat16 [49152, 2048], P(('sp', 'tp'))
All inputs are finite; a program needn't handle non-finite values.
Results may differ from a plain program's by a relative error of at most 0.012.
The roundings to bfloat16 on the way count: a program that leaves them out, or rounds other values in their place, can miss the bound.
Values may be sent and summed in bfloat16 or wider, within the bound.
A program may use at most 64 MiB of HBM per device.

v0:
```python
import functools

import jax
import jax.numpy as jnp
import numpy as np
from jax import lax
from jax.experimental import pallas as pl
from jax.experimental.pallas import tpu as pltpu
from jax.sharding import PartitionSpec as P

QUERY_HEADS = 16
KEY_VALUE_HEADS = 8
HEAD_DIM = 128
WINDOW_REACH = 128
GRID_W = 64
NORM_EPS = 1e-05
MASKED_SCORE = -1e30
LANES = 128
QUAD = 4
MESH = pl.DeviceIdType.MESH
F32 = jnp.float32
BF16 = jnp.bfloat16


def tile_of(extent, most):
    tile = min(extent, most)
    while extent % tile:
        tile -= LANES
    return tile


def block_kernel(
    n_sp,
    n_tp,
    cond_ref,
    ctx_cond_ref,
    gain_ref,
    cos_ref,
    sin_ref,
    sink_ref,
    latent_hbm,
    context_hbm,
    shift_hbm,
    scale_hbm,
    gate_hbm,
    wq_hbm,
    wk_hbm,
    wv_hbm,
    wo_hbm,
    out_ref,
    latent,
    context,
    shift_w,
    scale_w,
    gate_w,
    wq,
    wk,
    wv,
    wo,
    part,
    gathered,
    full,
    mod,
    hidden,
    ctx_hidden,
    queries,
    kv,
    ctx_kv,
    attended,
    partial_out,
    partial_in,
    own_total,
    load_sem,
    rs_send,
    rs_recv,
    ag_send,
    ag_recv,
    tp_send,
    tp_recv,
    hid_send,
    hid_recv,
    ctx_send,
    ctx_recv,
    halo_send,
    halo_recv,
    out_send,
    out_recv,
):
    sp = lax.axis_index("sp")
    tp = lax.axis_index("tp")
    rows, width = latent.shape
    group_rows = rows * n_tp
    columns = shift_w.shape[1]
    chunks = columns // LANES
    per = part.shape[1]
    query_width = wq.shape[1]
    pair = wk.shape[1]
    kv_local = pair // HEAD_DIM
    per_group = query_width // pair
    ctx_rows = context.shape[0]

    loads = [
        pltpu.make_async_copy(src, dst, load_sem.at[i])
        for i, (src, dst) in enumerate(
            [
                (shift_hbm, shift_w),
                (scale_hbm, scale_w),
                (gate_hbm, gate_w),
                (context_hbm, context),
                (latent_hbm, latent),
                (wk_hbm, wk),
                (wv_hbm, wv),
                (wq_hbm, wq),
                (wo_hbm, wo),
            ]
        )
    ]
    for load in loads:
        load.start()

    barrier = pltpu.get_barrier_semaphore()

    def greet_sp(d, carry):
        pl.semaphore_signal(
            barrier, inc=1, device_id={"sp": lax.rem(sp + d, n_sp)}, device_id_type=MESH
        )
        return carry

    def greet_tp(d, carry):
        pl.semaphore_signal(
            barrier, inc=1, device_id={"tp": lax.rem(tp + d, n_tp)}, device_id_type=MESH
        )
        return carry

    lax.fori_loop(1, n_sp, greet_sp, 0)
    lax.fori_loop(1, n_tp, greet_tp, 0)

    def silu(v):
        return v / (1.0 + jnp.exp(-v))

    depth = cond_ref.shape[1]
    row_id = lax.broadcasted_iota(jnp.int32, (16, depth), 0)
    active = jnp.where(
        row_id == 0,
        jnp.broadcast_to(silu(cond_ref[...]), (16, depth)),
        jnp.broadcast_to(silu(ctx_cond_ref[...]), (16, depth)),
    ).astype(BF16)
    part[...] = jnp.zeros_like(part)
    vector = 0
    for load, weight, count in zip(loads[:3], (shift_w, scale_w, gate_w), (2, 2, 1)):
        load.wait()
        product = jnp.dot(active, weight[...], preferred_element_type=F32)
        for v in range(count):
            for j in range(chunks):
                g = vector * chunks + j
                part[g // per, g % per : g % per + 1, :] = product[
                    v : v + 1, j * LANES : (j + 1) * LANES
                ]
            vector += 1

    pl.semaphore_wait(barrier, n_sp + n_tp - 2)

    def rs_copy(d):
        peer = lax.rem(sp + d, n_sp)
        return pltpu.make_async_remote_copy(
            src_ref=part.at[peer],
            dst_ref=gathered.at[sp],
            send_sem=rs_send.at[peer],
            recv_sem=rs_recv.at[sp],
            device_id={"sp": peer},
            device_id_type=MESH,
        )

    def rs_arrival(d):
        peer = lax.rem(sp + d, n_sp)
        return pltpu.make_async_remote_copy(
            src_ref=part.at[peer],
            dst_ref=gathered.at[peer],
            send_sem=rs_send.at[peer],
            recv_sem=rs_recv.at[peer],
            device_id={"sp": peer},
            device_id_type=MESH,
        )

    def loop(low, high, f):
        def step(i, carry):
            f(i)
            return carry

        lax.fori_loop(low, high, step, 0)

    loop(1, n_sp, lambda d: rs_copy(d).start())
    gathered[sp] = part[sp]
    loop(1, n_sp, lambda d: rs_arrival(d).wait_recv())
    full[tp, sp] = jnp.sum(gathered[...], axis=0)

    def ag_copy(d):
        peer = lax.rem(sp + d, n_sp)
        return pltpu.make_async_remote_copy(
            src_ref=full.at[tp, sp],
            dst_ref=full.at[tp, sp],
            send_sem=ag_send.at[peer],
            recv_sem=ag_recv.at[sp],
            device_id={"sp": peer},
            device_id_type=MESH,
        )

    def ag_arrival(d):
        peer = lax.rem(sp + d, n_sp)
        return pltpu.make_async_remote_copy(
            src_ref=full.at[tp, sp],
            dst_ref=full.at[tp, peer],
            send_sem=ag_send.at[peer],
            recv_sem=ag_recv.at[peer],
            device_id={"sp": peer},
            device_id_type=MESH,
        )

    loop(1, n_sp, lambda d: ag_copy(d).start())
    loop(1, n_sp, lambda d: ag_arrival(d).wait_recv())

    def tp_copy(d, mine):
        peer = lax.rem(tp + d, n_tp)
        slot = tp if mine else peer
        return pltpu.make_async_remote_copy(
            src_ref=full.at[tp],
            dst_ref=full.at[slot],
            send_sem=tp_send.at[peer],
            recv_sem=tp_recv.at[slot],
            device_id={"tp": peer},
            device_id_type=MESH,
        )

    loop(1, n_tp, lambda d: tp_copy(d, True).start())
    loop(1, n_tp, lambda d: tp_copy(d, False).wait_recv())
    for t in range(n_tp):
        for v in range(5):
            for j in range(chunks):
                g = v * chunks + j
                column = t * columns + j * LANES
                mod[v : v + 1, column : column + LANES] = full[t, g // per, g % per : g % per + 1, :]
    gain = gain_ref[...]
    mod[2:3, :] = gain * (1.0 + mod[2:3, :])
    mod[3:4, :] = gain * (1.0 + mod[3:4, :])

    def normed(block, shift_row, scale_row):
        floats = block.astype(F32)
        inverse = lax.rsqrt(jnp.mean(floats * floats, axis=-1, keepdims=True) + NORM_EPS)
        return (
            floats * inverse * mod[scale_row : scale_row + 1, :] + mod[shift_row : shift_row + 1, :]
        ).astype(BF16)

    for load in loads[3:7]:
        load.wait()
    ctx_hidden[...] = normed(context[...], 1, 3)
    tile = tile_of(pair, 256)

    def ctx_project(j):
        at = pl.multiple_of(j * tile, tile)
        ctx_kv[sp, :, pl.ds(at, tile)] = jnp.dot(
            ctx_hidden[...], wk[:, pl.ds(at, tile)], preferred_element_type=F32
        ).astype(BF16)
        ctx_kv[sp, :, pl.ds(pl.multiple_of(pair + at, tile), tile)] = jnp.dot(
            ctx_hidden[...], wv[:, pl.ds(at, tile)], preferred_element_type=F32
        ).astype(BF16)

    loop(0, pair // tile, ctx_project)

    lines = n_sp // QUAD
    line, corner = sp // QUAD, lax.rem(sp, QUAD)

    def ctx_copy(slot, peer, sem):
        return pltpu.make_async_remote_copy(
            src_ref=ctx_kv.at[slot],
            dst_ref=ctx_kv.at[slot],
            send_sem=ctx_send.at[sem],
            recv_sem=ctx_recv.at[slot],
            device_id={"sp": peer},
            device_id_type=MESH,
        )

    ctx_sends = []

    def send_ctx(slot, peer):
        copy = ctx_copy(slot, peer, len(ctx_sends))
        copy.start()
        ctx_sends.append(copy)

    def send_quad(slot):
        for d in range(1, QUAD):
            send_ctx(slot, line * QUAD + lax.rem(corner + d, QUAD))

    for d in range(1, lines):
        send_ctx(sp, lax.rem(line + d, lines) * QUAD + corner)
    send_quad(sp)

    def relay(d):
        slot = lax.rem(line + lines - d, lines) * QUAD + corner
        ctx_copy(slot, sp, 0).wait_recv()
        send_quad(slot)

    strip = 32
    own_start = pl.multiple_of(tp * rows, strip)

    def norm_strip(i):
        at = pl.multiple_of(i * strip, strip)
        hidden[pl.ds(pl.multiple_of(own_start + at, strip), strip), :] = normed(
            latent[pl.ds(at, strip), :], 0, 2
        )

    loop(0, rows // strip, norm_strip)

    def hid_copy(d, mine):
        peer = lax.rem(tp + d, n_tp)
        slot = tp if mine else peer
        at = pl.multiple_of(slot * rows, strip)
        mine_at = pl.multiple_of(tp * rows, strip)
        return pltpu.make_async_remote_copy(
            src_ref=hidden.at[pl.ds(mine_at, rows)],
            dst_ref=hidden.at[pl.ds(at, rows)],
            send_sem=hid_send.at[peer],
            recv_sem=hid_recv.at[slot],
            device_id={"tp": peer},
            device_id_type=MESH,
        )

    loop(1, n_tp, lambda d: hid_copy(d, True).start())

    quarter = HEAD_DIM // 4
    lane = lax.broadcasted_iota(jnp.int32, (rows, HEAD_DIM), 1)
    low_half = lax.rem(lane, 2 * quarter) < quarter

    def turned(values, cosine, sine):
        pieces = []
        for h in range(values.shape[1] // HEAD_DIM):
            u = values[:, h * HEAD_DIM : (h + 1) * HEAD_DIM]
            other = jnp.where(
                low_half, pltpu.roll(u, HEAD_DIM - quarter, 1), pltpu.roll(u, quarter, 1)
            )
            pieces.append(u * cosine + other * sine)
        return jnp.concatenate(pieces, axis=1).astype(BF16)

    def project_kv(slot):
        at = pl.multiple_of(slot * rows, strip)
        source = pl.ds(at, rows)
        target = pl.ds(pl.multiple_of(WINDOW_REACH + at, strip), rows)

        def one(j):
            col = pl.multiple_of(j * tile, tile)
            keys = jnp.dot(hidden[source, :], wk[:, pl.ds(col, tile)], preferred_element_type=F32)
            kv[target, pl.ds(col, tile)] = turned(keys, cos_ref[source, :], sin_ref[source, :])
            values = jnp.dot(hidden[source, :], wv[:, pl.ds(col, tile)], preferred_element_type=F32)
            kv[target, pl.ds(pl.multiple_of(pair + col, tile), tile)] = values.astype(BF16)

        loop(0, pair // tile, one)

    def project_q(slot):
        source = pl.ds(pl.multiple_of(slot * rows, strip), rows)
        q_tile = tile_of(query_width, 256)

        def one(j):
            col = pl.multiple_of(j * q_tile, q_tile)
            q = jnp.dot(hidden[source, :], wq[:, pl.ds(col, q_tile)], preferred_element_type=F32)
            queries[source, pl.ds(col, q_tile)] = turned(q, cos_ref[source, :], sin_ref[source, :])

        loop(0, query_width // q_tile, one)

    project_kv(tp)
    loop(1, n_tp, lambda d: hid_copy(d, False).wait_recv())
    loop(1, n_tp, lambda d: project_kv(lax.rem(tp + d, n_tp)))

    def halo_copy(up):
        source = group_rows if up else WINDOW_REACH
        target = 0 if up else group_rows + WINDOW_REACH
        which = 0 if up else 1
        return pltpu.make_async_remote_copy(
            src_ref=kv.at[pl.ds(source, WINDOW_REACH)],
            dst_ref=kv.at[pl.ds(target, WINDOW_REACH)],
            send_sem=halo_send.at[which],
            recv_sem=halo_recv.at[which],
            device_id={"sp": lax.rem(sp + (1 if up else n_sp - 1), n_sp)},
            device_id_type=MESH,
        )

    has_next, has_last = sp < n_sp - 1, sp > 0

    @pl.when(has_next)
    def _():
        halo_copy(True).start()

    @pl.when(has_last)
    def _():
        halo_copy(False).start()

    @pl.when(jnp.logical_not(has_last))
    def _():
        kv[0:WINDOW_REACH, :] = jnp.zeros((WINDOW_REACH, 2 * pair), BF16)

    @pl.when(jnp.logical_not(has_next))
    def _():
        kv[group_rows + WINDOW_REACH :, :] = jnp.zeros((WINDOW_REACH, 2 * pair), BF16)

    loads[7].wait()
    order = list(range(1, lines))
    if order:
        relay(order[0])
    project_q(tp)
    for d in order[1:2]:
        relay(d)
    loop(1, n_tp, lambda d: project_q(lax.rem(tp + d, n_tp)))
    for d in order[2:]:
        relay(d)

    @pl.when(has_last)
    def _():
        halo_copy(True).wait_recv()

    @pl.when(has_next)
    def _():
        halo_copy(False).wait_recv()

    def quad_arrivals(i):
        for d in range(1, QUAD):
            slot = i * QUAD + lax.rem(corner + d, QUAD)
            ctx_copy(slot, sp, 0).wait_recv()

    loop(0, lines, quad_arrivals)

    span = 3 * WINDOW_REACH
    stacked = per_group * WINDOW_REACH
    log2e = 1.4426950408889634
    factor = HEAD_DIM ** (-0.5) * log2e
    total_rows = group_rows * n_sp
    ctx_total = n_sp * ctx_rows
    contract = (((1,), (1,)), ((), ()))

    def attend(block):
        begin = pl.multiple_of(block * WINDOW_REACH, WINDOW_REACH)
        here = pl.ds(begin, WINDOW_REACH)
        around = pl.ds(begin, span)
        query_at = lax.rem(
            lax.broadcasted_iota(jnp.int32, (stacked, span), 0), WINDOW_REACH
        ) + WINDOW_REACH
        key_at = lax.broadcasted_iota(jnp.int32, (stacked, span), 1)
        key_pos = sp * group_rows + begin - WINDOW_REACH + key_at
        allowed = (
            (jnp.abs(key_at - query_at) <= WINDOW_REACH) & (key_pos >= 0) & (key_pos < total_rows)
        )
        for h in range(kv_local):
            heads = [h * per_group + i for i in range(per_group)]
            cols = slice(h * HEAD_DIM, (h + 1) * HEAD_DIM)
            value_cols = slice(pair + h * HEAD_DIM, pair + (h + 1) * HEAD_DIM)
            q = jnp.concatenate(
                [queries[here, i * HEAD_DIM : (i + 1) * HEAD_DIM] for i in heads], axis=0
            )
            band = lax.dot_general(q, kv[around, cols], contract, preferred_element_type=F32)
            band = jnp.where(allowed, band * factor, MASKED_SCORE)
            ctx_keys = ctx_kv[:, :, cols].reshape(ctx_total, HEAD_DIM)
            ctx_values = ctx_kv[:, :, value_cols].reshape(ctx_total, HEAD_DIM)
            far = lax.dot_general(q, ctx_keys, contract, preferred_element_type=F32) * factor
            sink = jnp.concatenate(
                [jnp.full((WINDOW_REACH, 1), sink_ref[0, i] * log2e, F32) for i in heads], axis=0
            )
            top = jnp.maximum(
                jnp.maximum(
                    jnp.max(band, axis=-1, keepdims=True), jnp.max(far, axis=-1, keepdims=True)
                ),
                sink,
            )
            band_exp = jnp.exp2(band - top)
            far_exp = jnp.exp2(far - top)
            total = (
                jnp.sum(band_exp, axis=-1, keepdims=True)
                + jnp.sum(far_exp, axis=-1, keepdims=True)
                + jnp.exp2(sink - top)
            )
            mixed = jnp.dot(
                band_exp.astype(BF16), kv[around, value_cols], preferred_element_type=F32
            ) + jnp.dot(far_exp.astype(BF16), ctx_values, preferred_element_type=F32)
            mixed = (mixed / total).astype(BF16)
            for n, i in enumerate(heads):
                attended[here, i * HEAD_DIM : (i + 1) * HEAD_DIM] = mixed[
                    n * WINDOW_REACH : (n + 1) * WINDOW_REACH
                ]

    by_part = rows % WINDOW_REACH == 0
    part_blocks = rows // WINDOW_REACH

    def attend_part(slot):
        if by_part:
            loop(0, part_blocks, lambda b: attend(slot * part_blocks + b))

    if not by_part:
        loop(0, group_rows // WINDOW_REACH, attend)
    loads[8].wait()
    out_tile = tile_of(width, 256)

    def out_copy(d, mine):
        peer = lax.rem(tp + d, n_tp)
        slot = tp if mine else peer
        return pltpu.make_async_remote_copy(
            src_ref=partial_out.at[peer],
            dst_ref=partial_in.at[slot],
            send_sem=out_send.at[peer],
            recv_sem=out_recv.at[slot],
            device_id={"tp": peer},
            device_id_type=MESH,
        )

    def project_out(slot, store):
        source = pl.ds(pl.multiple_of(slot * rows, strip), rows)

        def one(j):
            cols = pl.ds(pl.multiple_of(j * out_tile, out_tile), out_tile)
            store(
                cols,
                jnp.dot(attended[source, :], wo[:, cols], preferred_element_type=F32).astype(BF16),
            )

        loop(0, width // out_tile, one)

    def peer_part(d):
        slot = lax.rem(tp + d, n_tp)
        attend_part(slot)

        def store(cols, value):
            partial_out[slot, :, cols] = value

        project_out(slot, store)
        out_copy(d, True).start()

    loop(1, n_tp, peer_part)
    attend_part(tp)

    def keep(cols, value):
        own_total[:, cols] = value.astype(F32)

    project_out(tp, keep)
    loop(1, n_tp, lambda d: out_copy(d, False).wait_recv())

    def finish(i):
        at = pl.ds(pl.multiple_of(i * strip, strip), strip)
        mixed = own_total[at, :]
        for d in range(1, n_tp):
            mixed = mixed + partial_in[lax.rem(tp + d, n_tp), at, :].astype(F32)
        out_ref[at, :] = (latent[at, :].astype(F32) + mod[4:5, :] * mixed).astype(BF16)

    loop(0, rows // strip, finish)

    loop(1, n_sp, lambda d: rs_copy(d).wait_send())
    loop(1, n_sp, lambda d: ag_copy(d).wait_send())
    loop(1, n_tp, lambda d: tp_copy(d, True).wait_send())
    loop(1, n_tp, lambda d: hid_copy(d, True).wait_send())
    loop(1, n_tp, lambda d: out_copy(d, True).wait_send())
    for copy in ctx_sends:
        copy.wait_send()

    @pl.when(has_next)
    def _():
        halo_copy(True).wait_send()

    @pl.when(has_last)
    def _():
        halo_copy(False).wait_send()


def angle_tables(total_rows):
    inv_freq = np.power(
        10000.0, -np.arange(0, HEAD_DIM // 2, 2, dtype=np.float64) / (HEAD_DIM // 2)
    ).astype(np.float32)

    def tables(count):
        angle = (np.arange(count, dtype=np.float32)[:, None] * inv_freq).astype(np.float64)
        cosine, sine = np.cos(angle), np.sin(angle)
        return (
            np.concatenate([cosine, cosine], axis=1).astype(np.float32),
            np.concatenate([-sine, sine], axis=1).astype(np.float32),
        )

    return tables(total_rows // GRID_W), tables(GRID_W)


def shards(
    n_sp,
    n_tp,
    latent,
    condition,
    context_condition,
    context,
    norm_gain,
    shift_weight,
    scale_weight,
    gate_weight,
    query_weight,
    key_matrix,
    value_matrix,
    sink_logit_head,
    out_weight,
):
    rows, width = latent.shape
    group_rows = rows * n_tp
    grid_rows = group_rows // GRID_W
    half = HEAD_DIM // 2
    by_row, by_col = angle_tables(group_rows * n_sp)
    first = lax.axis_index("sp") * grid_rows

    def table(row_table, col_table):
        part = lax.dynamic_slice_in_dim(jnp.asarray(row_table), first, grid_rows, 0)
        part = jnp.broadcast_to(part[:, None], (grid_rows, GRID_W, half))
        col = jnp.broadcast_to(jnp.asarray(col_table)[None], (grid_rows, GRID_W, half))
        return jnp.concatenate([part, col], axis=-1).reshape(group_rows, HEAD_DIM)

    cosine, sine = table(by_row[0], by_col[0]), table(by_row[1], by_col[1])
    columns = shift_weight.shape[1]
    groups = 5 * columns // LANES
    per = -(-groups // n_sp)
    query_width = query_weight.shape[1]
    pair = key_matrix.shape[1]
    ctx_rows = context.shape[0]
    lines = n_sp // QUAD
    ctx_sends = (lines - 1) + (QUAD - 1) * lines
    dma = pltpu.SemaphoreType.DMA
    vmem = pl.BlockSpec(memory_space=pltpu.VMEM)
    anywhere = pl.BlockSpec(memory_space=pl.ANY)

    def like(array):
        return pltpu.VMEM(array.shape, array.dtype)

    return pl.pallas_call(
        functools.partial(block_kernel, n_sp, n_tp),
        out_shape=jax.ShapeDtypeStruct((rows, width), BF16),
        in_specs=[vmem] * 5 + [pl.BlockSpec(memory_space=pltpu.SMEM)] + [anywhere] * 9,
        out_specs=vmem,
        scratch_shapes=[
            like(latent),
            like(context),
            like(shift_weight),
            like(scale_weight),
            like(gate_weight),
            like(query_weight),
            like(key_matrix),
            like(value_matrix),
            like(out_weight),
            pltpu.VMEM((n_sp, per, LANES), F32),
            pltpu.VMEM((n_sp, per, LANES), F32),
            pltpu.VMEM((n_tp, n_sp, per, LANES), F32),
            pltpu.VMEM((8, width), F32),
            pltpu.VMEM((group_rows, width), BF16),
            like(context),
            pltpu.VMEM((group_rows, query_width), BF16),
            pltpu.VMEM((group_rows + 2 * WINDOW_REACH, 2 * pair), BF16),
            pltpu.VMEM((n_sp, ctx_rows, 2 * pair), BF16),
            pltpu.VMEM((group_rows, query_width), BF16),
            pltpu.VMEM((n_tp, rows, width), BF16),
            pltpu.VMEM((n_tp, rows, width), BF16),
            pltpu.VMEM((rows, width), F32),
            dma((9,)),
            dma((n_sp,)),
            dma((n_sp,)),
            dma((n_sp,)),
            dma((n_sp,)),
            dma((n_tp,)),
            dma((n_tp,)),
            dma((n_tp,)),
            dma((n_tp,)),
            dma((ctx_sends,)),
            dma((n_sp,)),
            dma((2,)),
            dma((2,)),
            dma((n_tp,)),
            dma((n_tp,)),
        ],
        compiler_params=pltpu.CompilerParams(
            collective_id=0, has_side_effects=True, vmem_limit_bytes=63 * 1024 * 1024
        ),
    )(
        condition.reshape(1, -1),
        context_condition.reshape(1, -1),
        norm_gain.reshape(1, -1),
        cosine,
        sine,
        sink_logit_head.reshape(1, -1),
        latent,
        context,
        shift_weight,
        scale_weight,
        gate_weight,
        query_weight,
        key_matrix,
        value_matrix,
        out_weight,
    )


def solution(mesh):
    placed = (
        P(("sp", "tp"), None),
        P("sp"),
        P("sp"),
        P("sp", None),
        P(),
        P("sp", "tp"),
        P("sp", "tp"),
        P("sp", "tp"),
        P(None, "tp"),
        P(None, "tp"),
        P(None, "tp"),
        P("tp"),
        P("tp", None),
    )
    return jax.shard_map(
        functools.partial(shards, mesh.shape["sp"], mesh.shape["tp"]),
        mesh=mesh,
        in_specs=placed,
        out_specs=P(("sp", "tp"), None),
        check_vma=False,
    )
```

profile of v0, /device:TPU:1, one launch (start us, length us, event | category | flops | bytes accessed | tf_op | source)
XLA Modules:
  0.0 141.9 jit_solution(13222188363882209297)
XLA Ops:
  0.0 0.7 constant_dynamic-slice_fusion
  0.8 0.0 copy-start.1
  0.8 0.7 copy-done.1
  1.6 0.0 copy-start
  1.6 0.9 pad_maximum_fusion
  2.5 0.0 copy-done
  2.5 0.9 pad_maximum_fusion.1
  3.5 136.6 %shard_map.163 = bf16[96,2048]{1,0:T(8,128)(2,1)} custom-call(f32[1,32]{1,0:T(1,128)} %bitcast.9, f32[1,32]{1,0:T(1,128)} %bitcast.10, f32[1,2048]{1,0:T(1,128)} %bitcast.8, f32[768,128]{1,0:T(8,128)} %bitcast.6, f32[768,128]{1,0:T(8,128)} %bitcast.7, f32[1,2]{1,0:T(1,128)} %bitcast.11, bf16[96,2048]{1,0:T(8,128)(2,1)} %latent_hbm.1, ...), custom_call_target="tpu_custom_call" | custom-call | tf_op jit(solution)/shard_map/pallas_call | solution.py:629
  140.1 1.8 %copy.19 = bf16[96,2048]{1,0:T(8,128)(2,1)} copy(bf16[96,2048]{1,0:T(8,128)(2,1)} %shard_map.163) | data formatting | bytes 786432
  (4 shorter events, 0.1 us)
Async XLA Ops:
  0.8 0.8 copy-start.1
  1.6 0.9 copy-start
where the time goes:
time: 142 us
  Pallas kernels  137 us (96%)
  local copies, waits for them, and re-layouts  3.33 us (2%)
  other arithmetic  1.85 us (1%)
    pallas_call x1, Pallas kernels, shards(): pl.pallas_call(functools.partial(block_kernel, n_sp, n_tp), out_shape=jax...  137 us

commit v1 on v0

v1 whole, which is shorter than its diff:
```python
import functools

import jax
import jax.numpy as jnp
import numpy as np
from jax import lax
from jax.experimental import pallas as pl
from jax.experimental.pallas import tpu as pltpu
from jax.sharding import PartitionSpec as P

HEAD_DIM = 128
REACH = 128
GRID_W = 64
NORM_EPS = 1e-05
MASKED_SCORE = -1e30
LANES = 128
NY = 4
NX = 4
MESH = pl.DeviceIdType.MESH
F32 = jnp.float32
BF16 = jnp.bfloat16
LOG2E = 1.4426950408889634


def loop(low, high, f):
    def step(i, carry):
        f(i)
        return carry

    lax.fori_loop(low, high, step, 0)


def block_kernel(
    n_sp,
    n_tp,
    cond_hbm,
    ctx_cond_hbm,
    gain_hbm,
    sink_hbm,
    rot_row_hbm,
    rot_col_hbm,
    latent_hbm,
    context_hbm,
    shift_hbm,
    scale_hbm,
    gate_hbm,
    wq_hbm,
    wk_hbm,
    wv_hbm,
    wo_hbm,
    out_ref,
    cond,
    ctx_cond,
    gain,
    sink,
    rot_row,
    rot_col,
    cos,
    sin,
    context,
    shift_w,
    scale_w,
    gate_w,
    wq,
    wkv,
    wo,
    lat,
    y_in,
    z_in,
    full,
    mod,
    hidden,
    ctx_hidden,
    queries,
    kv,
    ctx_kv,
    att,
    give,
    pin,
    outx,
    relay_in,
    x_in,
    own_total,
    load_sem,
    y_send,
    y_recv,
    z_send,
    z_recv,
    tp_send,
    tp_recv,
    lat_send,
    lat_recv,
    ctx_send,
    ctx_recv,
    halo_send,
    halo_recv,
    give_send,
    give_recv,
    rel_send,
    rel_recv,
    xs_send,
    xs_recv,
):
    sp = lax.axis_index("sp")
    tp = lax.axis_index("tp")
    n_z = n_sp // NY
    z, y = sp // NY, lax.rem(sp, NY)
    x, core = tp // 2, lax.rem(tp, 2)
    other = 1 - core
    partner = 2 * x + other

    def at_x(dx, c):
        return 2 * lax.rem(x + dx, NX) + c

    slots, rows, width = lat.shape
    group_rows = rows * n_tp
    half = rows // 2
    columns = shift_w.shape[1]
    chunks = columns // LANES
    vecs = y_in.shape[1]
    ctx_rows = context.shape[0]
    has_next, has_last = sp < n_sp - 1, sp > 0

    barrier = pltpu.get_barrier_semaphore()

    def greet(**where):
        pl.semaphore_signal(barrier, inc=1, device_id=where, device_id_type=MESH)

    loop(1, n_z, lambda d: greet(sp=lax.rem(z + d, n_z) * NY + y))
    loop(1, n_tp, lambda d: greet(tp=lax.rem(tp + d, n_tp)))
    loop(1, NY, lambda d: greet(sp=z * NY + lax.rem(y + d, NY)))
    cross_next = has_next & (y == NY - 1)
    cross_last = has_last & (y == 0)

    @pl.when(cross_next)
    def _():
        greet(sp=lax.rem(sp + 1, n_sp))

    @pl.when(cross_last)
    def _():
        greet(sp=lax.rem(sp + n_sp - 1, n_sp))

    own_lat = lat.at[tp]
    loads = {}
    for i, (name, src, dst) in enumerate(
        [
            ("cond", cond_hbm, cond),
            ("ctx_cond", ctx_cond_hbm, ctx_cond),
            ("shift", shift_hbm, shift_w),
            ("scale", scale_hbm, scale_w),
            ("gate", gate_hbm, gate_w),
            ("lat", latent_hbm, own_lat),
            ("row", rot_row_hbm.at[sp], rot_row),
            ("col", rot_col_hbm, rot_col),
            ("gain", gain_hbm, gain),
            ("context", context_hbm, context),
            ("wk", wk_hbm, wkv.at[:, 0:HEAD_DIM]),
            ("wv", wv_hbm, wkv.at[:, HEAD_DIM : 2 * HEAD_DIM]),
            ("wq", wq_hbm, wq),
            ("wo", wo_hbm, wo),
            ("sink", sink_hbm, sink),
        ]
    ):
        loads[name] = pltpu.make_async_copy(src, dst, load_sem.at[i])
        loads[name].start()

    def rcopy(src, dst, ssem, rsem, **where):
        return pltpu.make_async_remote_copy(
            src_ref=src,
            dst_ref=dst,
            send_sem=ssem,
            recv_sem=rsem,
            device_id=where,
            device_id_type=MESH,
        )

    def silu(v):
        return v / (1.0 + jnp.exp(-v))

    loads["cond"].wait()
    loads["ctx_cond"].wait()
    depth = cond.shape[1]
    row_id = lax.broadcasted_iota(jnp.int32, (16, depth), 0)
    active = jnp.where(
        row_id == 0,
        jnp.broadcast_to(silu(cond[...]), (16, depth)),
        jnp.broadcast_to(silu(ctx_cond[...]), (16, depth)),
    ).astype(BF16)
    vector = 0
    for name, weight, count in (("shift", shift_w, 2), ("scale", scale_w, 2), ("gate", gate_w, 1)):
        loads[name].wait()
        product = jnp.dot(active, weight[...], preferred_element_type=F32)
        for v in range(count):
            for j in range(chunks):
                y_in[y, vector * chunks + j] = product[v : v + 1, j * LANES : (j + 1) * LANES]
            vector += 1

    loads["row"].wait()
    loads["col"].wait()
    for g in range(group_rows // GRID_W):
        cos[g * GRID_W : (g + 1) * GRID_W, :] = rot_row[g : g + 1, :] + rot_col[0:GRID_W, :]
        sin[g * GRID_W : (g + 1) * GRID_W, :] = (
            rot_row[16 + g : 17 + g, :] + rot_col[GRID_W : 2 * GRID_W, :]
        )
    loads["lat"].wait()

    pl.semaphore_wait(
        barrier,
        (n_z - 1)
        + (n_tp - 1)
        + (NY - 1)
        + cross_next.astype(jnp.int32)
        + cross_last.astype(jnp.int32),
    )

    def y_copy(d, mine):
        peer = lax.rem(y + d, NY)
        slot = y if mine else peer
        return rcopy(
            y_in.at[y], y_in.at[slot], y_send.at[peer], y_recv.at[slot], sp=z * NY + peer
        )

    for d in (2, 1, 3):
        y_copy(d, True).start()

    low, high = pl.ds(0, half), pl.ds(half, half)

    def lat_copy(slot, part, sem, to):
        piece = lat.at[slot, part]
        which = 0 if part is not high else 1
        return rcopy(piece, piece, lat_send.at[sem], lat_recv.at[slot, which], tp=to)

    whole = pl.ds(0, rows)
    xp, xm = at_x(1, core), at_x(3, core)
    far = at_x(2, core)
    lat_sends = [
        lat_copy(tp, low, 0, xp),
        lat_copy(tp, high, 1, xm),
        lat_copy(tp, high, 2, xp),
        lat_copy(tp, low, 3, xm),
        lat_copy(tp, low, 4, partner),
        lat_copy(tp, high, 5, partner),
    ]
    for copy in lat_sends:
        copy.start()

    def lat_arrival(slot, which):
        lat_copy(slot, low if which == 0 else high, 0, partner).wait_recv()

    loop(1, NY, lambda d: y_copy(d, False).wait_recv())
    z_in[z] = jnp.sum(y_in[...], axis=0)

    def z_copy(d, mine):
        peer = lax.rem(z + d, n_z)
        slot = z if mine else peer
        return rcopy(
            z_in.at[z], z_in.at[slot], z_send.at[peer], z_recv.at[slot], sp=peer * NY + y
        )

    def far_first(i):
        step = (i + 1) // 2
        return n_z // 2 + jnp.where(lax.rem(i, 2) == 1, step, -step)

    loop(0, n_z - 1, lambda i: z_copy(far_first(i), True).start())
    loop(1, n_z, lambda d: z_copy(d, False).wait_recv())
    full[tp] = jnp.sum(z_in[...], axis=0)

    def tp_copy(d, mine):
        peer = lax.rem(tp + d, n_tp)
        slot = tp if mine else peer
        return rcopy(full.at[tp], full.at[slot], tp_send.at[peer], tp_recv.at[slot], tp=peer)

    loop(1, n_tp, lambda d: tp_copy(d, True).start())

    lat_arrival(xm, 0)
    relay_a = lat_copy(xm, low, 6, xp)
    relay_a.start()
    lat_arrival(xp, 1)
    relay_b = lat_copy(xp, high, 7, xm)
    relay_b.start()
    lat_sends += [relay_a, relay_b]
    lat_arrival(xm, 1)
    lat_arrival(xp, 0)
    for i, slot in enumerate((xm, xp)):
        for j, part in enumerate((low, high)):
            copy = lat_copy(slot, part, 8 + 2 * i + j, partner)
            copy.start()
            lat_sends.append(copy)

    loop(1, n_tp, lambda d: tp_copy(d, False).wait_recv())
    for t in range(n_tp):
        for v in range(5):
            for j in range(chunks):
                column = t * columns + j * LANES
                mod[v : v + 1, column : column + LANES] = full[t, v * chunks + j]
    loads["gain"].wait()
    gains = gain[...]
    mod[2:3, :] = gains * (1.0 + mod[2:3, :])
    mod[3:4, :] = gains * (1.0 + mod[3:4, :])

    def normed(block, shift_row, scale_row):
        floats = block.astype(F32)
        inverse = lax.rsqrt(jnp.mean(floats * floats, axis=-1, keepdims=True) + NORM_EPS)
        return (
            floats * inverse * mod[scale_row : scale_row + 1, :] + mod[shift_row : shift_row + 1, :]
        ).astype(BF16)

    loads["context"].wait()
    loads["wk"].wait()
    loads["wv"].wait()
    ctx_hidden[...] = normed(context[...], 1, 3)
    ctx_kv[sp] = jnp.dot(ctx_hidden[...], wkv[...], preferred_element_type=F32).astype(BF16)

    def ctx_copy(slot, peer, sem):
        return rcopy(
            ctx_kv.at[slot], ctx_kv.at[slot], ctx_send.at[sem], ctx_recv.at[slot], sp=peer
        )

    def ctx_z(i):
        peer = lax.rem(z + far_first(i), n_z) * NY + y
        return ctx_copy(sp, peer, i)

    loop(0, n_z - 1, lambda i: ctx_z(i).start())

    def ctx_y(i, d):
        step = (i + 1) // 2
        slot = lax.rem(z + n_z + jnp.where(lax.rem(i, 2) == 1, step, -step), n_z) * NY + y
        return slot, ctx_copy(slot, z * NY + lax.rem(y + d, NY), n_z - 1 + 3 * i + d - 1)

    def relay_ctx(i):
        slot, _ = ctx_y(i, 1)

        @pl.when(i > 0)
        def _():
            ctx_copy(slot, sp, 0).wait_recv()

        for d in (2, 1, 3):
            ctx_y(i, d)[1].start()

    relay_ctx(jnp.int32(0))

    lane = lax.broadcasted_iota(jnp.int32, (2 * rows, HEAD_DIM), 1)
    quarter = HEAD_DIM // 4
    low_half = lax.rem(lane, 2 * quarter) < quarter
    strip = 32

    def turned(u, cosine, sine):
        swapped = jnp.where(
            low_half, pltpu.roll(u, HEAD_DIM - quarter, 1), pltpu.roll(u, quarter, 1)
        )
        return (u * cosine + swapped * sine).astype(BF16)

    def process(chip):
        def norm_strip(i):
            for c in range(2):
                at = pl.multiple_of(i * strip, strip)
                hidden[pl.ds(pl.multiple_of(c * rows + at, strip), strip), :] = normed(
                    lat[2 * chip + c, pl.ds(at, strip), :], 0, 2
                )

        loop(0, rows // strip, norm_strip)
        begin = pl.multiple_of(chip * 2 * rows, strip)
        here = pl.ds(begin, 2 * rows)
        kept = pl.ds(pl.multiple_of(begin + REACH, strip), 2 * rows)
        cosine, sine = cos[here, :], sin[here, :]
        pair = jnp.dot(hidden[...], wkv[...], preferred_element_type=F32)
        kv[kept, 0:HEAD_DIM] = turned(pair[:, 0:HEAD_DIM], cosine, sine)
        kv[kept, HEAD_DIM:] = pair[:, HEAD_DIM:].astype(BF16)
        q = jnp.dot(hidden[...], wq[...], preferred_element_type=F32)
        for h in range(2):
            cols = slice(h * HEAD_DIM, (h + 1) * HEAD_DIM)
            queries[here, cols] = turned(q[:, cols], cosine, sine)

    loads["wq"].wait()

    def stage(k):
        chip = lax.rem(x + jnp.where(k == 1, 3, jnp.where(k == 2, 1, k - jnp.where(k == 3, 1, 0))), NX)
        slot = 2 * chip + other

        @pl.when(k == 3)
        def _():
            mine = 2 * chip + core
            lat_arrival(mine, 0)
            lat_copy(mine, low, 12, partner).start()
            lat_arrival(mine, 1)
            lat_copy(mine, high, 13, partner).start()
            loop(3, 7, relay_ctx)

        lat_arrival(slot, 0)
        lat_arrival(slot, 1)
        process(chip)

        @pl.when(k == 2)
        def _():
            loop(1, 3, relay_ctx)

    loop(0, 4, stage)
    lat_sends += [lat_copy(far, low, 12, partner), lat_copy(far, high, 13, partner)]

    def halo_copy(up):
        source = group_rows if up else REACH
        target = 0 if up else group_rows + REACH
        which = 0 if up else 1
        return rcopy(
            kv.at[pl.ds(source, REACH)],
            kv.at[pl.ds(target, REACH)],
            halo_send.at[which],
            halo_recv.at[which],
            sp=lax.rem(sp + (1 if up else n_sp - 1), n_sp),
        )

    @pl.when(has_next)
    def _():
        halo_copy(True).start()

    @pl.when(has_last)
    def _():
        halo_copy(False).start()

    @pl.when(jnp.logical_not(has_last))
    def _():
        kv[0:REACH, :] = jnp.zeros((REACH, 2 * HEAD_DIM), BF16)

    @pl.when(jnp.logical_not(has_next))
    def _():
        kv[group_rows + REACH :, :] = jnp.zeros((REACH, 2 * HEAD_DIM), BF16)

    loop(7, n_z, relay_ctx)

    loads["wo"].wait()
    loads["sink"].wait()

    @pl.when(has_last)
    def _():
        halo_copy(True).wait_recv()

    @pl.when(has_next)
    def _():
        halo_copy(False).wait_recv()

    def quad_arrivals(i):
        for d in range(1, NY):
            ctx_copy(i * NY + lax.rem(y + d, NY), sp, 0).wait_recv()

    loop(0, n_z, quad_arrivals)

    span = rows + 2 * REACH
    total_rows = group_rows * n_sp
    ctx_total = n_sp * ctx_rows
    factor = HEAD_DIM ** (-0.5) * LOG2E
    contract = (((1,), (1,)), ((), ()))

    def attend(slot):
        begin = pl.multiple_of(slot * rows, strip)
        here = pl.ds(begin, rows)
        around = pl.ds(begin, span)
        query_at = lax.rem(lax.broadcasted_iota(jnp.int32, (2 * rows, span), 0), rows) + REACH
        key_at = lax.broadcasted_iota(jnp.int32, (2 * rows, span), 1)
        key_pos = sp * group_rows + begin - REACH + key_at
        allowed = (jnp.abs(key_at - query_at) <= REACH) & (key_pos >= 0) & (key_pos < total_rows)
        q = jnp.concatenate([queries[here, 0:HEAD_DIM], queries[here, HEAD_DIM:]], axis=0)
        band = lax.dot_general(q, kv[around, 0:HEAD_DIM], contract, preferred_element_type=F32)
        band = jnp.where(allowed, band * factor, MASKED_SCORE)
        ctx_keys = ctx_kv[:, :, 0:HEAD_DIM].reshape(ctx_total, HEAD_DIM)
        ctx_values = ctx_kv[:, :, HEAD_DIM:].reshape(ctx_total, HEAD_DIM)
        far_logits = lax.dot_general(q, ctx_keys, contract, preferred_element_type=F32) * factor
        sinks = jnp.concatenate(
            [jnp.broadcast_to(sink[0:1, i : i + 1] * LOG2E, (rows, 1)) for i in range(2)], axis=0
        )
        top = jnp.maximum(
            jnp.maximum(
                jnp.max(band, axis=-1, keepdims=True), jnp.max(far_logits, axis=-1, keepdims=True)
            ),
            sinks,
        )
        band_exp = jnp.exp2(band - top)
        far_exp = jnp.exp2(far_logits - top)
        total = (
            jnp.sum(band_exp, axis=-1, keepdims=True)
            + jnp.sum(far_exp, axis=-1, keepdims=True)
            + jnp.exp2(sinks - top)
        )
        mixed = jnp.dot(
            band_exp.astype(BF16), kv[around, HEAD_DIM:], preferred_element_type=F32
        ) + jnp.dot(far_exp.astype(BF16), ctx_values, preferred_element_type=F32)
        mixed = (mixed / total).astype(BF16)
        for h in range(2):
            att[:, h * HEAD_DIM : (h + 1) * HEAD_DIM] = mixed[h * rows : (h + 1) * rows]

    def chip_of(k):
        return lax.rem(
            x + jnp.where(k == 0, 2, jnp.where(k == 1, 1, jnp.where(k == 2, 3, 0))), NX
        )

    def give_copy(k):
        return rcopy(give.at[k], pin.at[k], give_send.at[k], give_recv.at[k], tp=partner)

    def relay_copy(up):
        part, i, to = (low, 0, xp) if up else (high, 1, xm)
        return rcopy(outx.at[0, part], relay_in.at[i], rel_send.at[i], rel_recv.at[i], tp=to)

    def x_copy(i):
        part = high if i in (0, 3) else low
        side = i // 2
        return rcopy(
            outx.at[1 + side, part],
            x_in.at[side, part],
            xs_send.at[i],
            xs_recv.at[i],
            tp=xm if side else xp,
        )

    n_tile = 512

    def project(store):
        for j in range(width // n_tile):
            cols = slice(j * n_tile, (j + 1) * n_tile)
            store(cols, jnp.dot(att[...], wo[:, cols], preferred_element_type=F32))

    def sub_block(j):
        keep = (j == 2) | (j == 4) | (j == 6) | (j == 7)
        k = jnp.where(
            keep, jnp.where(j == 7, 3, (j - 2) // 2), jnp.where(j == 0, 0, (j + 1) // 2)
        )
        attend(2 * chip_of(k) + jnp.where(keep, core, other))

        @pl.when(jnp.logical_not(keep))
        def _():
            def store(cols, value):
                give[k, :, cols] = value.astype(BF16)

            project(store)
            give_copy(k).start()

        @pl.when(keep)
        def _():
            give_copy(k).wait_recv()

        @pl.when(keep & (j < 7))
        def _():
            def store(cols, value):
                outx[k, :, cols] = (value + pin[k, :, cols].astype(F32)).astype(BF16)

            project(store)

        @pl.when(j == 2)
        def _():
            relay_copy(True).start()
            relay_copy(False).start()

        @pl.when(j == 4)
        def _():
            x_copy(0).start()

        @pl.when(j == 6)
        def _():
            x_copy(2).start()

        @pl.when(j == 7)
        def _():
            def store(cols, value):
                own_total[:, cols] = value + pin[3, :, cols].astype(F32)

            project(store)

    loop(0, 8, sub_block)

    for up, i in ((True, 1), (False, 3)):
        part, side = (low, 0) if up else (high, 1)
        relay_copy(up).wait_recv()
        for s in range(half // 16):
            at = pl.ds((0 if up else half) + 16 * s, 16)
            outx[1 + side, at, :] = (
                outx[1 + side, at, :].astype(F32)
                + relay_in[side, pl.ds(16 * s, 16), :].astype(F32)
            ).astype(BF16)
        x_copy(i).start()

    for i in range(4):
        x_copy(i).wait_recv()

    def finish(i):
        at = pl.ds(pl.multiple_of(i * strip, strip), strip)
        mixed = own_total[at, :] + x_in[0, at, :].astype(F32) + x_in[1, at, :].astype(F32)
        out_ref[at, :] = (lat[tp, at, :].astype(F32) + mod[4:5, :] * mixed).astype(BF16)

    loop(0, rows // strip, finish)

    loop(1, NY, lambda d: y_copy(d, True).wait_send())
    loop(1, n_z, lambda d: z_copy(d, True).wait_send())
    loop(1, n_tp, lambda d: tp_copy(d, True).wait_send())
    for copy in lat_sends:
        copy.wait_send()
    loop(0, n_z - 1, lambda i: ctx_z(i).wait_send())

    def ctx_drain(i):
        for d in range(1, NY):
            ctx_y(i, d)[1].wait_send()

    loop(0, n_z, ctx_drain)
    loop(0, 4, lambda k: give_copy(k).wait_send())
    for up in (True, False):
        relay_copy(up).wait_send()
    for i in range(4):
        x_copy(i).wait_send()

    @pl.when(has_next)
    def _():
        halo_copy(True).wait_send()

    @pl.when(has_last)
    def _():
        halo_copy(False).wait_send()


def angle_tables(total_rows, n_sp):
    inv_freq = np.power(
        10000.0, -np.arange(0, HEAD_DIM // 2, 2, dtype=np.float64) / (HEAD_DIM // 2)
    ).astype(np.float32)

    def tables(count):
        angle = (np.arange(count, dtype=np.float32)[:, None] * inv_freq).astype(np.float64)
        cosine, sine = np.cos(angle), np.sin(angle)
        return (
            np.concatenate([cosine, cosine], axis=1).astype(np.float32),
            np.concatenate([-sine, sine], axis=1).astype(np.float32),
        )

    half = HEAD_DIM // 2
    grid_rows = total_rows // GRID_W
    per = grid_rows // n_sp
    by_row, by_col = tables(grid_rows), tables(GRID_W)
    rows = np.zeros((n_sp, 32, HEAD_DIM), np.float32)
    rows[:, 0:per, :half] = by_row[0].reshape(n_sp, per, half)
    rows[:, 16 : 16 + per, :half] = by_row[1].reshape(n_sp, per, half)
    cols = np.zeros((2 * GRID_W, HEAD_DIM), np.float32)
    cols[:GRID_W, half:] = by_col[0]
    cols[GRID_W:, half:] = by_col[1]
    return rows, cols


def shards(
    n_sp,
    n_tp,
    latent,
    condition,
    context_condition,
    context,
    norm_gain,
    shift_weight,
    scale_weight,
    gate_weight,
    query_weight,
    key_matrix,
    value_matrix,
    sink_logit_head,
    out_weight,
):
    rows, width = latent.shape
    group_rows = rows * n_tp
    rot_rows, rot_cols = angle_tables(group_rows * n_sp, n_sp)
    columns = shift_weight.shape[1]
    groups = 5 * columns // LANES
    query_width = query_weight.shape[1]
    ctx_rows = context.shape[0]
    n_z = n_sp // NY
    dma = pltpu.SemaphoreType.DMA
    vmem = pl.BlockSpec(memory_space=pltpu.VMEM)
    anywhere = pl.BlockSpec(memory_space=pl.ANY)
    half = rows // 2

    def like(array):
        return pltpu.VMEM(array.shape, array.dtype)

    condition = condition.reshape(1, -1)
    context_condition = context_condition.reshape(1, -1)
    norm_gain = norm_gain.reshape(1, -1)
    sink = sink_logit_head.reshape(1, -1)
    return pl.pallas_call(
        functools.partial(block_kernel, n_sp, n_tp),
        out_shape=jax.ShapeDtypeStruct((rows, width), BF16),
        in_specs=[anywhere] * 15,
        out_specs=vmem,
        scratch_shapes=[
            like(condition),
            like(context_condition),
            like(norm_gain),
            like(sink),
            pltpu.VMEM((32, HEAD_DIM), F32),
            pltpu.VMEM((2 * GRID_W, HEAD_DIM), F32),
            pltpu.VMEM((group_rows, HEAD_DIM), F32),
            pltpu.VMEM((group_rows, HEAD_DIM), F32),
            like(context),
            like(shift_weight),
            like(scale_weight),
            like(gate_weight),
            like(query_weight),
            pltpu.VMEM((width, 2 * HEAD_DIM), BF16),
            like(out_weight),
            pltpu.VMEM((n_tp, rows, width), BF16),
            pltpu.VMEM((NY, groups, 1, LANES), F32),
            pltpu.VMEM((n_z, groups, 1, LANES), F32),
            pltpu.VMEM((n_tp, groups, 1, LANES), F32),
            pltpu.VMEM((8, width), F32),
            pltpu.VMEM((2 * rows, width), BF16),
            like(context),
            pltpu.VMEM((group_rows, query_width), BF16),
            pltpu.VMEM((group_rows + 2 * REACH, 2 * HEAD_DIM), BF16),
            pltpu.VMEM((n_sp, ctx_rows, 2 * HEAD_DIM), BF16),
            pltpu.VMEM((rows, query_width), BF16),
            pltpu.VMEM((4, rows, width), BF16),
            pltpu.VMEM((4, rows, width), BF16),
            pltpu.VMEM((3, rows, width), BF16),
            pltpu.VMEM((2, half, width), BF16),
            pltpu.VMEM((2, rows, width), BF16),
            pltpu.VMEM((rows, width), F32),
            dma((15,)),
            dma((NY,)),
            dma((NY,)),
            dma((n_z,)),
            dma((n_z,)),
            dma((n_tp,)),
            dma((n_tp,)),
            dma((14,)),
            dma((n_tp, 2)),
            dma((n_z - 1 + 3 * n_z,)),
            dma((n_sp,)),
            dma((2,)),
            dma((2,)),
            dma((4,)),
            dma((4,)),
            dma((2,)),
            dma((2,)),
            dma((4,)),
            dma((4,)),
        ],
        compiler_params=pltpu.CompilerParams(
            collective_id=0, has_side_effects=True, vmem_limit_bytes=60 * 1024 * 1024
        ),
    )(
        condition,
        context_condition,
        norm_gain,
        sink,
        jnp.asarray(rot_rows),
        jnp.asarray(rot_cols),
        latent,
        context,
        shift_weight,
        scale_weight,
        gate_weight,
        query_weight,
        key_matrix,
        value_matrix,
        out_weight,
    )


def solution(mesh):
    placed = (
        P(("sp", "tp"), None),
        P("sp"),
        P("sp"),
        P("sp", None),
        P(),
        P("sp", "tp"),
        P("sp", "tp"),
        P("sp", "tp"),
        P(None, "tp"),
        P(None, "tp"),
        P(None, "tp"),
        P("tp"),
        P("tp", None),
    )
    return jax.shard_map(
        functools.partial(shards, mesh.shape["sp"], mesh.shape["tp"]),
        mesh=mesh,
        in_specs=placed,
        out_specs=P(("sp", "tp"), None),
        check_vma=False,
    )
```

time: 142 us -> 72.7 us (0.51)
  Pallas kernels: 137 us -> 70.8 us
  other arithmetic: 1.85 us -> 0 us
  local copies, waits for them, and re-layouts: 3.33 us -> 1.77 us
    pallas_call x1, Pallas kernels: 137 us -> 70.8 us  [shards(): pl.pallas_call(functools.partial(block_kernel, n_sp, n_tp), out_shape=jax...]
    concatenate x2 -> x0, other arithmetic: 1.85 us -> none  [table(): return jnp.concatenate([part, col], axis=-1).reshape(group_rows, HEAD_DIM)]
where the time goes in v1:
time: 72.7 us; the launch traced here: 72.6 us
  Pallas kernels  70.8 us (97%)
  local copies, waits for them, and re-layouts  1.77 us (2%)
    pallas_call x1, Pallas kernels, shards(): pl.pallas_call(functools.partial(block_kernel, n_sp, n_tp), out_shape=jax...  70.8 us
    unnamed x1, local copies, waits for them, and re-layouts  1.77 us

profile of v1, /device:TPU:1, one launch (start us, length us, event | category | flops | bytes accessed | tf_op | source)
XLA Modules:
  0.0 72.6 jit_solution(16792468611108676989)
XLA Ops:
  0.0 70.8 %shard_map.145 = bf16[96,2048]{1,0:T(8,128)(2,1)} custom-call(f32[1,32]{1,0:T(1,128)} %bitcast.5, f32[1,32]{1,0:T(1,128)} %bitcast.6, f32[1,2048]{1,0:T(1,128)} %bitcast.4, f32[1,2]{1,0:T(1,128)} %bitcast.7, f32[64,32,128]{2,1,0:T(8,128)} %constant.4.clone.rot_row_hbm, f32[128,128]{1,0:T(8,128)} %constant.5.clone.rot_col_hbm, bf16[96,2048]{1,0:T(8,128)(2,1)} %latent_hbm.1, ...), custom_call_target="tpu_custom_call" | custom-call | tf_op jit(solution)/shard_map/pallas_call | solution.py:679
  70.8 1.8 %copy.17 = bf16[96,2048]{1,0:T(8,128)(2,1)} copy(bf16[96,2048]{1,0:T(8,128)(2,1)} %shard_map.145) | data formatting | bytes 786432

commit v2 on v1

v2 whole, which is shorter than its diff:
```python
import functools

import jax
import jax.numpy as jnp
import numpy as np
from jax import lax
from jax.experimental import pallas as pl
from jax.experimental.pallas import tpu as pltpu
from jax.sharding import PartitionSpec as P

HEAD_DIM = 128
REACH = 128
GRID_W = 64
NORM_EPS = 1e-05
MASKED_SCORE = -1e30
LANES = 128
NY = 4
NX = 4
MESH = pl.DeviceIdType.MESH
F32 = jnp.float32
BF16 = jnp.bfloat16
LOG2E = 1.4426950408889634


def loop(low, high, f):
    def step(i, carry):
        f(i)
        return carry

    lax.fori_loop(low, high, step, 0)


def block_kernel(
    n_sp,
    n_tp,
    cond_hbm,
    ctx_cond_hbm,
    gain_hbm,
    sink_hbm,
    rot_row_hbm,
    rot_col_hbm,
    latent_hbm,
    context_hbm,
    shift_hbm,
    scale_hbm,
    gate_hbm,
    wq_hbm,
    wk_hbm,
    wv_hbm,
    wo_hbm,
    out_ref,
    cond,
    ctx_cond,
    gain,
    sink,
    rot_row,
    rot_col,
    cos,
    sin,
    context,
    shift_w,
    scale_w,
    gate_w,
    wq,
    wkv,
    wo,
    lat,
    z_in,
    full,
    inv,
    mod,
    hidden,
    ctx_hidden,
    queries,
    kv,
    ctx_kv,
    att,
    give,
    pin,
    outx,
    relay_in,
    x_in,
    kept,
    bias,
    load_sem,
    z_send,
    z_recv,
    xy_send,
    xy_recv,
    lat_send,
    lat_recv,
    ctx_send,
    ctx_recv,
    halo_send,
    halo_recv,
    give_send,
    give_recv,
    rel_send,
    rel_recv,
    xs_send,
    xs_recv,
):
    sp = lax.axis_index("sp")
    tp = lax.axis_index("tp")
    n_z = n_sp // NY
    z, x = sp // NY, tp // 2
    y, core = sp - NY * z, tp - 2 * x
    other = 1 - core
    partner = 2 * x + other

    def wrap(i, n):
        return jnp.where(i >= n, i - n, i)

    def at_x(dx, c):
        return 2 * wrap(x + dx, NX) + c

    slots, rows, width = lat.shape
    group_rows = rows * n_tp
    half = rows // 2
    columns = shift_w.shape[1]
    chunks = columns // LANES
    ctx_rows = context.shape[0]
    has_next, has_last = sp < n_sp - 1, sp > 0

    barrier = pltpu.get_barrier_semaphore()

    def greet(**where):
        pl.semaphore_signal(barrier, inc=1, device_id=where, device_id_type=MESH)

    zs = [wrap(z + d, n_z) for d in range(n_z)]
    ys = [wrap(y + d, NY) for d in range(NY)]
    tps = [wrap(tp + d, n_tp) for d in range(n_tp)]
    z_steps = (4, n_z - 4, 2, n_z - 2, 1, n_z - 1)
    for d in z_steps:
        greet(sp=zs[d] * NY + y)

    def plane(d):
        return z * NY + ys[d // n_tp], tps[d % n_tp]

    for d in range(1, NY * n_tp):
        to_sp, to_tp = plane(d)
        greet(sp=to_sp, tp=to_tp)
    cross_next = has_next & (y == NY - 1)
    cross_last = has_last & (y == 0)

    @pl.when(cross_next)
    def _():
        greet(sp=lax.rem(sp + 1, n_sp))

    @pl.when(cross_last)
    def _():
        greet(sp=lax.rem(sp + n_sp - 1, n_sp))

    own_lat = lat.at[tp]
    loads = {}
    for i, (name, src, dst) in enumerate(
        [
            ("cond", cond_hbm, cond),
            ("ctx_cond", ctx_cond_hbm, ctx_cond),
            ("shift", shift_hbm, shift_w),
            ("scale", scale_hbm, scale_w),
            ("gate", gate_hbm, gate_w),
            ("lat", latent_hbm, own_lat),
            ("row", rot_row_hbm.at[sp], rot_row),
            ("col", rot_col_hbm, rot_col),
            ("gain", gain_hbm, gain),
            ("context", context_hbm, context),
            ("wk", wk_hbm, wkv.at[:, 0:HEAD_DIM]),
            ("wv", wv_hbm, wkv.at[:, HEAD_DIM : 2 * HEAD_DIM]),
            ("wq", wq_hbm, wq),
            ("wo", wo_hbm, wo),
            ("sink", sink_hbm, sink),
        ]
    ):
        loads[name] = pltpu.make_async_copy(src, dst, load_sem.at[i])
        loads[name].start()

    def rcopy(src, dst, ssem, rsem, **where):
        return pltpu.make_async_remote_copy(
            src_ref=src,
            dst_ref=dst,
            send_sem=ssem,
            recv_sem=rsem,
            device_id=where,
            device_id_type=MESH,
        )

    def silu(v):
        return v / (1.0 + jnp.exp(-v))

    loads["cond"].wait()
    loads["ctx_cond"].wait()
    depth = cond.shape[1]
    row_id = lax.broadcasted_iota(jnp.int32, (16, depth), 0)
    active = jnp.where(
        row_id == 0,
        jnp.broadcast_to(silu(cond[...]), (16, depth)),
        jnp.broadcast_to(silu(ctx_cond[...]), (16, depth)),
    ).astype(BF16)
    vector = 0
    for name, weight, count in (("shift", shift_w, 2), ("scale", scale_w, 2), ("gate", gate_w, 1)):
        loads[name].wait()
        product = jnp.dot(active, weight[...], preferred_element_type=F32)
        for v in range(count):
            for j in range(chunks):
                z_in[0, vector * chunks + j] = product[v : v + 1, j * LANES : (j + 1) * LANES]
            vector += 1

    loads["row"].wait()
    loads["col"].wait()
    for g in range(group_rows // GRID_W):
        cos[g * GRID_W : (g + 1) * GRID_W, :] = rot_row[g : g + 1, :] + rot_col[0:GRID_W, :]
        sin[g * GRID_W : (g + 1) * GRID_W, :] = (
            rot_row[16 + g : 17 + g, :] + rot_col[GRID_W : 2 * GRID_W, :]
        )
    def mask_rows(i):
        at = pl.ds(pl.multiple_of(i * 64, 64), 64)
        shape = (64, 4 * rows)
        lane_at = lax.rem(lax.broadcasted_iota(jnp.int32, shape, 1), 2 * rows)
        row = lane_at + jnp.where(lane_at < rows, other * rows, (core - 1) * rows)
        key = lax.broadcasted_iota(jnp.int32, shape, 0) + i * 64
        bias[at, :] = jnp.where(jnp.abs(key - row - REACH) <= REACH, 0.0, MASKED_SCORE)

    loop(0, (2 * rows + 2 * REACH) // 64, mask_rows)
    loads["lat"].wait()

    pl.semaphore_wait(
        barrier,
        len(z_steps)
        + (NY * n_tp - 1)
        + cross_next.astype(jnp.int32)
        + cross_last.astype(jnp.int32),
    )

    def z_copy(source, slot, step, stage):
        return rcopy(
            z_in.at[source],
            z_in.at[slot],
            z_send.at[0],
            z_recv.at[stage],
            sp=zs[step] * NY + y,
        )

    def z_wait(stage, count):
        got = z_in.at[pl.ds(0, count)]
        rcopy(got, got, z_send.at[0], z_recv.at[stage], sp=sp).wait_recv()

    z_copy(0, 3, n_z - 2, 0).start()
    z_copy(0, 1, 1, 0).start()
    z_copy(0, 2, n_z - 1, 0).start()

    low, high = pl.ds(0, half), pl.ds(half, half)

    def lat_copy(slot, part, sem, to):
        piece = lat.at[slot, part]
        which = 0 if part is not high else 1
        return rcopy(piece, piece, lat_send.at[0], lat_recv.at[slot, which], tp=to)

    whole = pl.ds(0, rows)
    xp, xm = at_x(1, core), at_x(3, core)
    far = at_x(2, core)
    for copy in (
        lat_copy(tp, low, 0, xp),
        lat_copy(tp, high, 1, xm),
        lat_copy(tp, low, 4, partner),
        lat_copy(tp, high, 5, partner),
    ):
        copy.start()

    def lat_arrival(slot, which):
        lat_copy(slot, low if which == 0 else high, 0, partner).wait_recv()

    def invert(slot):
        floats = lat[slot].astype(F32)
        mean = jnp.mean(floats * floats, axis=-1, keepdims=True)
        inv[slot] = jnp.broadcast_to(lax.rsqrt(mean + NORM_EPS), (rows, LANES))

    z_wait(0, 3)
    z_in[4] = (z_in[0] + z_in[1]) + (z_in[2] + z_in[3])
    z_copy(4, 5, 2, 1).start()
    z_copy(4, 6, n_z - 2, 1).start()
    invert(tp)
    z_wait(1, 2)
    z_in[7] = z_in[5] + z_in[6]
    z_copy(7, 8, 4, 2).start()
    z_copy(7, 9, n_z - 4, 2).start()
    lat_arrival(partner, 0)
    lat_arrival(partner, 1)
    invert(partner)
    z_wait(2, 2)
    own_full = y * n_tp + tp
    full[own_full] = z_in[8] + z_in[9]

    def xy_copy(d, mine):
        to_sp, to_tp = plane(d)
        peer = ys[d // n_tp] * n_tp + to_tp
        slot = own_full if mine else peer
        return rcopy(
            full.at[own_full],
            full.at[slot],
            xy_send.at[0],
            xy_recv.at[0],
            sp=to_sp,
            tp=to_tp,
        )

    for d in range(1, NY * n_tp):
        xy_copy(d, True).start()

    for part, i, to in ((high, 2, xp), (low, 3, xm)):
        copy = lat_copy(tp, part, i, to)
        copy.start()

    for i, slot, order in ((0, xm, (0,)), (1, xp, (1,))):
        for j in order:
            part = (low, high)[j]
            lat_arrival(slot, j)
            copy = lat_copy(slot, part, 8 + 2 * i + j, partner)
            copy.start()
    xy_all = full.at[pl.ds(0, NY * n_tp - 1)]
    xy_total = rcopy(xy_all, xy_all, xy_send.at[0], xy_recv.at[0], sp=sp)
    xy_total.wait_recv()
    for t in range(n_tp):
        sums = full[t]
        for r in range(1, NY):
            sums = sums + full[r * n_tp + t]
        for v in range(5):
            for j in range(chunks):
                column = t * columns + j * LANES
                mod[v : v + 1, column : column + LANES] = sums[v * chunks + j]
    loads["gain"].wait()
    gains = gain[...]
    mod[2:3, :] = gains * (1.0 + mod[2:3, :])
    mod[3:4, :] = gains * (1.0 + mod[3:4, :])

    def normed(block, shift_row, scale_row):
        floats = block.astype(F32)
        inverse = lax.rsqrt(jnp.mean(floats * floats, axis=-1, keepdims=True) + NORM_EPS)
        return (
            floats * inverse * mod[scale_row : scale_row + 1, :] + mod[shift_row : shift_row + 1, :]
        ).astype(BF16)

    loads["context"].wait()
    loads["wk"].wait()
    loads["wv"].wait()
    ctx_hidden[...] = normed(context[...], 1, 3)
    ctx_kv[sp] = jnp.dot(ctx_hidden[...], wkv[...], preferred_element_type=F32).astype(BF16)

    def ctx_copy(slot, peer, sem):
        return rcopy(
            ctx_kv.at[slot], ctx_kv.at[slot], ctx_send.at[0], ctx_recv.at[sem], sp=peer
        )

    def near_first(i):
        return i // 2 + 1 if i % 2 == 0 else n_z - i // 2 - 1

    def ctx_z(i):
        return ctx_copy(sp, zs[near_first(i)] * NY + y, z)

    for i in range(n_z - 1):
        ctx_z(i).start()

    relay_a = lat_copy(xm, low, 6, xp)
    relay_a.start()
    relay_b = lat_copy(xp, high, 7, xm)
    relay_b.start()

    def ctx_y(i, d):
        slot = (zs[near_first(i - 1)] if i else z) * NY + y
        return slot, ctx_copy(slot, z * NY + ys[d], n_z)

    def relay_ctx(first, last):
        for i in range(first, last):
            if i:
                of = zs[near_first(i - 1)]
                ctx_copy(of * NY + y, sp, of).wait_recv()
            for d in (2, 1, 3):
                ctx_y(i, d)[1].start()

    relay_ctx(0, 1)

    lane = lax.broadcasted_iota(jnp.int32, (2 * rows, HEAD_DIM), 1)
    quarter = HEAD_DIM // 4
    low_half = lax.rem(lane, 2 * quarter) < quarter
    strip = 32

    def turned(u, cosine, sine):
        swapped = jnp.where(
            low_half, pltpu.roll(u, HEAD_DIM - quarter, 1), pltpu.roll(u, quarter, 1)
        )
        return (u * cosine + swapped * sine).astype(BF16)

    def halo_copy(up):
        source = group_rows if up else REACH
        target = 0 if up else group_rows + REACH
        which = 0 if up else 1
        return rcopy(
            kv.at[pl.ds(source, REACH)],
            kv.at[pl.ds(target, REACH)],
            halo_send.at[which],
            halo_recv.at[which],
            sp=lax.rem(sp + (1 if up else n_sp - 1), n_sp),
        )

    def process(chip, relay_one, relay_two):

        def norm_strip(i):
            at = pl.ds(pl.multiple_of(i * strip, strip), strip)
            for c in range(2):
                inverse = inv[2 * chip + c, at, :]
                to = pl.ds(pl.multiple_of(c * rows + i * strip, strip), strip)
                for j in range(width // LANES):
                    cols = slice(j * LANES, (j + 1) * LANES)
                    hidden[to, cols] = (
                        lat[2 * chip + c, at, cols].astype(F32) * inverse * mod[2:3, cols]
                        + mod[0:1, cols]
                    ).astype(BF16)

        loop(0, rows // strip, norm_strip)
        relay_ctx(*relay_one)
        begin = pl.multiple_of(chip * 2 * rows, strip)
        here = pl.ds(begin, 2 * rows)
        kept = pl.ds(pl.multiple_of(begin + REACH, strip), 2 * rows)
        cosine, sine = cos[here, :], sin[here, :]
        pair = jnp.dot(hidden[...], wkv[...], preferred_element_type=F32)
        kv[kept, 0:HEAD_DIM] = turned(pair[:, 0:HEAD_DIM], cosine, sine)
        kv[kept, HEAD_DIM:] = pair[:, HEAD_DIM:].astype(BF16)
        q = jnp.dot(hidden[...], wq[...], preferred_element_type=F32)
        for h in range(2):
            cols = slice(h * HEAD_DIM, (h + 1) * HEAD_DIM)
            queries[here, cols] = turned(q[:, cols], cosine, sine)

        @pl.when(has_next & (chip == NX - 1))
        def _():
            halo_copy(True).start()

        @pl.when(has_last & (chip == 0))
        def _():
            halo_copy(False).start()

        relay_ctx(*relay_two)

    loads["wq"].wait()

    near = jnp.where(x < 2, NX - 1, 1)

    polls = [((0, 0), (0, 0)), ((1, 3), (3, 5)), ((5, 7), (7, 9)), ((0, 0), (0, 0))]
    for k in range(NX):
        step = (0, near, NX - near, 2)[k]
        chip = lax.rem(x + step, NX)
        slot = 2 * chip + other
        if k == 1:
            for i, neighbour, j in ((0, xm, 1), (1, xp, 0)):
                part = (low, high)[j]
                lat_arrival(neighbour, j)
                copy = lat_copy(neighbour, part, 8 + 2 * i + j, partner)
                copy.start()
            invert(xm)
            invert(xp)
        if k == 3:
            lat_arrival(far, 0)
            lat_copy(far, low, 12, partner).start()
            lat_arrival(far, 1)
            lat_copy(far, high, 13, partner).start()
            invert(far)
            relay_ctx(9, n_z)
        if k:
            lat_arrival(slot, 0)
            lat_arrival(slot, 1)
            invert(slot)
        process(chip, *polls[k])


    @pl.when(jnp.logical_not(has_last))
    def _():
        kv[0:REACH, :] = jnp.zeros((REACH, 2 * HEAD_DIM), BF16)

    @pl.when(jnp.logical_not(has_next))
    def _():
        kv[group_rows + REACH :, :] = jnp.zeros((REACH, 2 * HEAD_DIM), BF16)

    loads["wo"].wait()
    loads["sink"].wait()

    @pl.when(has_last)
    def _():
        halo_copy(True).wait_recv()

    @pl.when(has_next)
    def _():
        halo_copy(False).wait_recv()

    rest = ctx_kv.at[pl.ds(0, n_z * (NY - 1))]
    rcopy(rest, rest, ctx_send.at[0], ctx_recv.at[n_z], sp=sp).wait_recv()

    span = 2 * rows + 2 * REACH
    across = (((0,), (0,)), ((), ()))
    total_rows = group_rows * n_sp
    ctx_total = n_sp * ctx_rows
    factor = HEAD_DIM ** (-0.5) * LOG2E
    contract = (((1,), (1,)), ((), ()))

    both = 2 * rows
    lanes = 2 * both

    def attend(chip):
        begin = pl.multiple_of(chip * both, strip)
        around = pl.ds(begin, span)
        given = pl.ds(pl.multiple_of(begin + other * rows, strip), rows)
        kept_at = pl.ds(pl.multiple_of(begin + core * rows, strip), rows)
        q = jnp.concatenate(
            [
                queries[at, h * HEAD_DIM : (h + 1) * HEAD_DIM]
                for h in range(2)
                for at in (given, kept_at)
            ],
            axis=0,
        )
        key_pos = (
            sp * group_rows + begin - REACH + lax.broadcasted_iota(jnp.int32, (span, lanes), 0)
        )
        outside = (key_pos < 0) | (key_pos >= total_rows)
        band = lax.dot_general(kv[around, 0:HEAD_DIM], q, contract, preferred_element_type=F32)
        band = jnp.where(outside, MASKED_SCORE, band * factor + bias[...])
        ctx_keys = ctx_kv[:, :, 0:HEAD_DIM].reshape(ctx_total, HEAD_DIM)
        ctx_values = ctx_kv[:, :, HEAD_DIM:].reshape(ctx_total, HEAD_DIM)
        far_logits = lax.dot_general(ctx_keys, q, contract, preferred_element_type=F32) * factor
        sinks = jnp.concatenate(
            [jnp.broadcast_to(sink[0:1, i : i + 1] * LOG2E, (1, both)) for i in range(2)], axis=1
        )
        top = jnp.maximum(
            jnp.maximum(
                jnp.max(band, axis=0, keepdims=True), jnp.max(far_logits, axis=0, keepdims=True)
            ),
            sinks,
        )
        band_exp = jnp.exp2(band - top)
        far_exp = jnp.exp2(far_logits - top)
        total = (
            jnp.sum(band_exp, axis=0, keepdims=True)
            + jnp.sum(far_exp, axis=0, keepdims=True)
            + jnp.exp2(sinks - top)
        )
        mixed = lax.dot_general(
            kv[around, HEAD_DIM:], band_exp.astype(BF16), across, preferred_element_type=F32
        ) + lax.dot_general(
            ctx_values, far_exp.astype(BF16), across, preferred_element_type=F32
        )
        mixed = (mixed / total).T.astype(BF16)
        for h in range(2):
            att[:, h * HEAD_DIM : (h + 1) * HEAD_DIM] = mixed[h * both : (h + 1) * both]

    def chip_of(k):
        return lax.rem(
            x + jnp.where(k == 0, 2, jnp.where(k == 1, 1, jnp.where(k == 2, 3, 0))), NX
        )

    def give_copy(k):
        return rcopy(give.at[k], pin.at[k], give_send.at[0], give_recv.at[k], tp=partner)

    def relay_copy(up):
        part, i, to = (low, 0, xp) if up else (high, 1, xm)
        return rcopy(outx.at[0, part], relay_in.at[i], rel_send.at[0], rel_recv.at[i], tp=to)

    def x_copy(i):
        part = high if i in (0, 3) else low
        side = i // 2
        return rcopy(
            outx.at[1 + side, part],
            x_in.at[side, part],
            xs_send.at[0],
            xs_recv.at[0],
            tp=xm if side else xp,
        )

    n_tile = width

    def project(k):
        for first, store in ((0, "give"), (rows, "keep")):
            for j in range(width // n_tile):
                cols = slice(j * n_tile, (j + 1) * n_tile)
                value = jnp.dot(
                    att[first : first + rows, :], wo[:, cols], preferred_element_type=F32
                )
                if store == "give":
                    give[k, :, cols] = value.astype(BF16)
                else:
                    kept[:, cols] = value
            if store == "give":
                give_copy(k).start()

    def add_given(k, store):
        give_copy(k).wait_recv()

        def one(i):
            at = pl.ds(pl.multiple_of(i * strip, strip), strip)
            store(at, kept[at, :] + pin[k, at, :].astype(F32))

        loop(0, rows // strip, one)

    def chip_block(k):
        attend(chip_of(k))

        @pl.when(k > 0)
        def _():
            def store(at, value):
                outx[k - 1, at, :] = value.astype(BF16)

            add_given(k - 1, store)

        @pl.when(k == 1)
        def _():
            relay_copy(True).start()
            relay_copy(False).start()

        @pl.when(k == 2)
        def _():
            x_copy(0).start()

        @pl.when(k == 3)
        def _():
            x_copy(2).start()

        project(k)

    loop(0, NX, chip_block)

    for up, i in ((True, 1), (False, 3)):
        part, side = (low, 0) if up else (high, 1)
        relay_copy(up).wait_recv()
        for s in range(half // 16):
            at = pl.ds((0 if up else half) + 16 * s, 16)
            outx[1 + side, at, :] = (
                outx[1 + side, at, :].astype(F32)
                + relay_in[side, pl.ds(16 * s, 16), :].astype(F32)
            ).astype(BF16)
        x_copy(i).start()

    def own_store(at, value):
        kept[at, :] = value

    add_given(NX - 1, own_store)
    z_sent = z_in.at[pl.ds(0, 7)]
    rcopy(z_sent, z_sent, z_send.at[0], z_recv.at[0], sp=sp).wait_send()
    xy_total.wait_send()
    sent = lat.at[pl.ds(0, 7)]
    rcopy(sent, sent, lat_send.at[0], lat_recv.at[0, 0], sp=sp).wait_send()
    sent = ctx_kv.at[pl.ds(0, n_z * NY - 1)]
    rcopy(sent, sent, ctx_send.at[0], ctx_recv.at[0], sp=sp).wait_send()

    @pl.when(has_next)
    def _():
        halo_copy(True).wait_send()

    @pl.when(has_last)
    def _():
        halo_copy(False).wait_send()

    def whole_copy(ref, ssem, rsem):
        return rcopy(ref, ref, ssem, rsem, sp=sp)

    whole_copy(x_in, xs_send.at[0], xs_recv.at[0]).wait_recv()

    def finish(i):
        at = pl.ds(pl.multiple_of(i * strip, strip), strip)
        mixed = kept[at, :] + x_in[0, at, :].astype(F32) + x_in[1, at, :].astype(F32)
        out_ref[at, :] = (lat[tp, at, :].astype(F32) + mod[4:5, :] * mixed).astype(BF16)

    loop(0, rows // strip, finish)

    whole_copy(give, give_send.at[0], give_recv.at[0]).wait_send()
    whole_copy(outx.at[0], rel_send.at[0], rel_recv.at[0]).wait_send()
    whole_copy(outx.at[pl.ds(1, 2)], xs_send.at[0], xs_recv.at[0]).wait_send()


def angle_tables(total_rows, n_sp):
    inv_freq = np.power(
        10000.0, -np.arange(0, HEAD_DIM // 2, 2, dtype=np.float64) / (HEAD_DIM // 2)
    ).astype(np.float32)

    def tables(count):
        angle = (np.arange(count, dtype=np.float32)[:, None] * inv_freq).astype(np.float64)
        cosine, sine = np.cos(angle), np.sin(angle)
        return (
            np.concatenate([cosine, cosine], axis=1).astype(np.float32),
            np.concatenate([-sine, sine], axis=1).astype(np.float32),
        )

    half = HEAD_DIM // 2
    grid_rows = total_rows // GRID_W
    per = grid_rows // n_sp
    by_row, by_col = tables(grid_rows), tables(GRID_W)
    rows = np.zeros((n_sp, 32, HEAD_DIM), np.float32)
    rows[:, 0:per, :half] = by_row[0].reshape(n_sp, per, half)
    rows[:, 16 : 16 + per, :half] = by_row[1].reshape(n_sp, per, half)
    cols = np.zeros((2 * GRID_W, HEAD_DIM), np.float32)
    cols[:GRID_W, half:] = by_col[0]
    cols[GRID_W:, half:] = by_col[1]
    return rows, cols


def shards(
    n_sp,
    n_tp,
    latent,
    condition,
    context_condition,
    context,
    norm_gain,
    shift_weight,
    scale_weight,
    gate_weight,
    query_weight,
    key_matrix,
    value_matrix,
    sink_logit_head,
    out_weight,
):
    rows, width = latent.shape
    group_rows = rows * n_tp
    rot_rows, rot_cols = angle_tables(group_rows * n_sp, n_sp)
    columns = shift_weight.shape[1]
    groups = 5 * columns // LANES
    query_width = query_weight.shape[1]
    ctx_rows = context.shape[0]
    n_z = n_sp // NY
    dma = pltpu.SemaphoreType.DMA
    vmem = pl.BlockSpec(memory_space=pltpu.VMEM)
    anywhere = pl.BlockSpec(memory_space=pltpu.HBM)
    half = rows // 2

    def like(array):
        return pltpu.VMEM(array.shape, array.dtype)

    condition = condition.reshape(1, -1)
    context_condition = context_condition.reshape(1, -1)
    norm_gain = norm_gain.reshape(1, -1)
    sink = sink_logit_head.reshape(1, -1)
    return pl.pallas_call(
        functools.partial(block_kernel, n_sp, n_tp),
        out_shape=pltpu.VMEM((rows, width), BF16),
        in_specs=[anywhere] * 15,
        out_specs=vmem,
        scratch_shapes=[
            like(condition),
            like(context_condition),
            like(norm_gain),
            like(sink),
            pltpu.VMEM((32, HEAD_DIM), F32),
            pltpu.VMEM((2 * GRID_W, HEAD_DIM), F32),
            pltpu.VMEM((group_rows, HEAD_DIM), F32),
            pltpu.VMEM((group_rows, HEAD_DIM), F32),
            like(context),
            like(shift_weight),
            like(scale_weight),
            like(gate_weight),
            like(query_weight),
            pltpu.VMEM((width, 2 * HEAD_DIM), BF16),
            like(out_weight),
            pltpu.VMEM((n_tp, rows, width), BF16),
            pltpu.VMEM((10, groups, 1, LANES), F32),
            pltpu.VMEM((NY * n_tp, groups, 1, LANES), F32),
            pltpu.VMEM((n_tp, rows, LANES), F32),
            pltpu.VMEM((8, width), F32),
            pltpu.VMEM((2 * rows, width), BF16),
            like(context),
            pltpu.VMEM((group_rows, query_width), BF16),
            pltpu.VMEM((group_rows + 2 * REACH, 2 * HEAD_DIM), BF16),
            pltpu.VMEM((n_sp, ctx_rows, 2 * HEAD_DIM), BF16),
            pltpu.VMEM((2 * rows, query_width), BF16),
            pltpu.VMEM((4, rows, width), BF16),
            pltpu.VMEM((4, rows, width), BF16),
            pltpu.VMEM((3, rows, width), BF16),
            pltpu.VMEM((2, half, width), BF16),
            pltpu.VMEM((2, rows, width), BF16),
            pltpu.VMEM((rows, width), F32),
            pltpu.VMEM((2 * rows + 2 * REACH, 4 * rows), F32),
            dma((15,)),
            dma((1,)),
            dma((3,)),
            dma((1,)),
            dma((1,)),
            dma((1,)),
            dma((n_tp, 2)),
            dma((1,)),
            dma((n_z + 1,)),
            dma((2,)),
            dma((2,)),
            dma((1,)),
            dma((4,)),
            dma((1,)),
            dma((2,)),
            dma((1,)),
            dma((1,)),
        ],
        compiler_params=pltpu.CompilerParams(
            collective_id=0, has_side_effects=True, vmem_limit_bytes=int(60 * 1024 * 1024)
        ),
    )(
        condition,
        context_condition,
        norm_gain,
        sink,
        jnp.asarray(rot_rows),
        jnp.asarray(rot_cols),
        latent,
        context,
        shift_weight,
        scale_weight,
        gate_weight,
        query_weight,
        key_matrix,
        value_matrix,
        out_weight,
    )


def solution(mesh):
    placed = (
        P(("sp", "tp"), None),
        P("sp"),
        P("sp"),
        P("sp", None),
        P(),
        P("sp", "tp"),
        P("sp", "tp"),
        P("sp", "tp"),
        P(None, "tp"),
        P(None, "tp"),
        P(None, "tp"),
        P("tp"),
        P("tp", None),
    )
    return jax.shard_map(
        functools.partial(shards, mesh.shape["sp"], mesh.shape["tp"]),
        mesh=mesh,
        in_specs=placed,
        out_specs=P(("sp", "tp"), None),
        check_vma=False,
    )
```

time: 72.7 us -> 67.2 us (0.924)
  Pallas kernels: 70.8 us -> 66.3 us
  local copies, waits for them, and re-layouts: 1.77 us -> 0.75 us
    pallas_call x1, Pallas kernels: 70.8 us -> 66.3 us  [shards(): pl.pallas_call(functools.partial(block_kernel, n_sp, n_tp), out_shape=plt...]
    unnamed x1, local copies, waits for them, and re-layouts: 1.77 us -> 0.75 us
where the time goes in v2:
time: 67.2 us; the launch traced here: 67.1 us
  Pallas kernels  66.3 us (99%)
  local copies, waits for them, and re-layouts  0.75 us (1%)
    pallas_call x1, Pallas kernels, shards(): pl.pallas_call(functools.partial(block_kernel, n_sp, n_tp), out_shape=plt...  66.3 us

profile of v2, /device:TPU:1, one launch (start us, length us, event | category | flops | bytes accessed | tf_op | source)
XLA Modules:
  0.0 67.1 jit_solution(9535040950306086072)
XLA Ops:
  0.0 66.3 %shard_map.145 = bf16[96,2048]{1,0:T(8,128)(2,1)S(1)} custom-call(f32[1,32]{1,0:T(1,128)} %bitcast.5, f32[1,32]{1,0:T(1,128)} %bitcast.6, f32[1,2048]{1,0:T(1,128)} %bitcast.4, f32[1,2]{1,0:T(1,128)} %bitcast.7, f32[64,32,128]{2,1,0:T(8,128)} %constant.4.clone.rot_row_hbm, f32[128,128]{1,0:T(8,128)} %constant.5.clone.rot_col_hbm, ...), custom_call_target="tpu_custom_call" | custom-call | tf_op jit(solution)/shard_map/pallas_call | solution.py:739
  66.3 0.7 %copy.17 = bf16[96,2048]{1,0:T(8,128)(2,1)} copy(bf16[96,2048]{1,0:T(8,128)(2,1)S(1)} %shard_map.145) | data formatting | bytes 786432

commit v3 on v2

--- a/solution.py
+++ b/solution.py
@@ -78,10 +78,13 @@
     give,
     pin,
     outx,
-    relay_in,
     x_in,
+    att_out,
+    att_in,
+    wo_far,
     kept,
     bias,
+    edge,
     load_sem,
     z_send,
     z_recv,
@@ -95,10 +98,12 @@
     halo_recv,
     give_send,
     give_recv,
-    rel_send,
-    rel_recv,
     xs_send,
     xs_recv,
+    att_send,
+    att_recv,
+    wf_send,
+    wf_recv,
 ):
     sp = lax.axis_index("sp")
     tp = lax.axis_index("tp")
@@ -130,8 +135,10 @@
     zs = [wrap(z + d, n_z) for d in range(n_z)]
     ys = [wrap(y + d, NY) for d in range(NY)]
     tps = [wrap(tp + d, n_tp) for d in range(n_tp)]
-    z_steps = (4, n_z - 4, 2, n_z - 2, 1, n_z - 1)
-    for d in z_steps:
+    far_first = [
+        n_z // 2 + ((i + 1) // 2 if i % 2 else -((i + 1) // 2)) for i in range(n_z - 1)
+    ]
+    for d in far_first:
         greet(sp=zs[d] * NY + y)
 
     def plane(d):
@@ -203,51 +210,26 @@
         product = jnp.dot(active, weight[...], preferred_element_type=F32)
         for v in range(count):
             for j in range(chunks):
-                z_in[0, vector * chunks + j] = product[v : v + 1, j * LANES : (j + 1) * LANES]
+                z_in[z, vector * chunks + j] = product[v : v + 1, j * LANES : (j + 1) * LANES]
             vector += 1
 
-    loads["row"].wait()
-    loads["col"].wait()
-    for g in range(group_rows // GRID_W):
-        cos[g * GRID_W : (g + 1) * GRID_W, :] = rot_row[g : g + 1, :] + rot_col[0:GRID_W, :]
-        sin[g * GRID_W : (g + 1) * GRID_W, :] = (
-            rot_row[16 + g : 17 + g, :] + rot_col[GRID_W : 2 * GRID_W, :]
-        )
-    def mask_rows(i):
-        at = pl.ds(pl.multiple_of(i * 64, 64), 64)
-        shape = (64, 4 * rows)
-        lane_at = lax.rem(lax.broadcasted_iota(jnp.int32, shape, 1), 2 * rows)
-        row = lane_at + jnp.where(lane_at < rows, other * rows, (core - 1) * rows)
-        key = lax.broadcasted_iota(jnp.int32, shape, 0) + i * 64
-        bias[at, :] = jnp.where(jnp.abs(key - row - REACH) <= REACH, 0.0, MASKED_SCORE)
-
-    loop(0, (2 * rows + 2 * REACH) // 64, mask_rows)
     loads["lat"].wait()
 
     pl.semaphore_wait(
         barrier,
-        len(z_steps)
+        (n_z - 1)
         + (NY * n_tp - 1)
         + cross_next.astype(jnp.int32)
         + cross_last.astype(jnp.int32),
     )
 
-    def z_copy(source, slot, step, stage):
+    def z_copy(d, slot):
         return rcopy(
-            z_in.at[source],
-            z_in.at[slot],
-            z_send.at[0],
-            z_recv.at[stage],
-            sp=zs[step] * NY + y,
-        )
-
-    def z_wait(stage, count):
-        got = z_in.at[pl.ds(0, count)]
-        rcopy(got, got, z_send.at[0], z_recv.at[stage], sp=sp).wait_recv()
-
-    z_copy(0, 3, n_z - 2, 0).start()
-    z_copy(0, 1, 1, 0).start()
-    z_copy(0, 2, n_z - 1, 0).start()
+            z_in.at[z], z_in.at[slot], z_send.at[0], z_recv.at[0], sp=zs[d] * NY + y
+        )
+
+    for d in far_first:
+        z_copy(d, z).start()
 
     low, high = pl.ds(0, half), pl.ds(half, half)
 
@@ -275,21 +257,50 @@
         mean = jnp.mean(floats * floats, axis=-1, keepdims=True)
         inv[slot] = jnp.broadcast_to(lax.rsqrt(mean + NORM_EPS), (rows, LANES))
 
-    z_wait(0, 3)
-    z_in[4] = (z_in[0] + z_in[1]) + (z_in[2] + z_in[3])
-    z_copy(4, 5, 2, 1).start()
-    z_copy(4, 6, n_z - 2, 1).start()
+    wo_part = wo.shape[0] // NY // 2
+
+    def far_weights(source, to_sp, to_tp, piece, sem):
+        at = pl.ds(pl.multiple_of((2 * y + piece) * wo_part, wo_part), wo_part)
+        return rcopy(
+            source.at[at], wo_far.at[at], wf_send.at[0], wf_recv.at[sem], sp=to_sp, tp=to_tp
+        )
+
+    def share_far_weights(piece):
+        far_weights(wo, sp, far, piece, piece).wait_recv()
+        for d in (2, 1, 3):
+            far_weights(wo_far, z * NY + ys[d], tp, piece, 2 + piece).start()
+
+    loads["wo"].wait()
+    far_weights(wo, sp, far, 0, 0).start()
+
+    def rotary_and_mask():
+        loads["row"].wait()
+        loads["col"].wait()
+        for g in range(group_rows // GRID_W):
+            cos[g * GRID_W : (g + 1) * GRID_W, :] = rot_row[g : g + 1, :] + rot_col[0:GRID_W, :]
+            sin[g * GRID_W : (g + 1) * GRID_W, :] = (
+                rot_row[16 + g : 17 + g, :] + rot_col[GRID_W : 2 * GRID_W, :]
+            )
+        def mask_rows(i):
+            at = pl.ds(pl.multiple_of(i * 64, 64), 64)
+            shape = (64, 4 * rows)
+            lane_at = lax.rem(lax.broadcasted_iota(jnp.int32, shape, 1), 2 * rows)
+            row = lane_at + jnp.where(lane_at < rows, other * rows, (core - 1) * rows)
+            key = lax.broadcasted_iota(jnp.int32, shape, 0) + i * 64
+            bias[at, :] = jnp.where(jnp.abs(key - row - REACH) <= REACH, 0.0, MASKED_SCORE)
+
+        loop(0, (2 * rows + 2 * REACH) // 64, mask_rows)
+
+    rotary_and_mask()
     invert(tp)
-    z_wait(1, 2)
-    z_in[7] = z_in[5] + z_in[6]
-    z_copy(7, 8, 4, 2).start()
-    z_copy(7, 9, n_z - 4, 2).start()
     lat_arrival(partner, 0)
     lat_arrival(partner, 1)
     invert(partner)
-    z_wait(2, 2)
+    z_all = z_in.at[pl.ds(0, n_z - 1)]
+    z_total = rcopy(z_all, z_all, z_send.at[0], z_recv.at[0], sp=sp)
+    z_total.wait_recv()
     own_full = y * n_tp + tp
-    full[own_full] = z_in[8] + z_in[9]
+    full[own_full] = jnp.sum(z_in[...], axis=0)
 
     def xy_copy(d, mine):
         to_sp, to_tp = plane(d)
@@ -311,12 +322,15 @@
         copy = lat_copy(tp, part, i, to)
         copy.start()
 
+    far_weights(wo, sp, far, 1, 1).start()
+
     for i, slot, order in ((0, xm, (0,)), (1, xp, (1,))):
         for j in order:
             part = (low, high)[j]
             lat_arrival(slot, j)
             copy = lat_copy(slot, part, 8 + 2 * i + j, partner)
             copy.start()
+    share_far_weights(0)
     xy_all = full.at[pl.ds(0, NY * n_tp - 1)]
     xy_total = rcopy(xy_all, xy_all, xy_send.at[0], xy_recv.at[0], sp=sp)
     xy_total.wait_recv()
@@ -479,7 +493,6 @@
     def _():
         kv[group_rows + REACH :, :] = jnp.zeros((REACH, 2 * HEAD_DIM), BF16)
 
-    loads["wo"].wait()
     loads["sink"].wait()
 
     @pl.when(has_last)
@@ -492,6 +505,8 @@
 
     rest = ctx_kv.at[pl.ds(0, n_z * (NY - 1))]
     rcopy(rest, rest, ctx_send.at[0], ctx_recv.at[n_z], sp=sp).wait_recv()
+
+    share_far_weights(1)
 
     span = 2 * rows + 2 * REACH
     across = (((0,), (0,)), ((), ()))
@@ -517,36 +532,50 @@
             axis=0,
         )
         key_pos = (
-            sp * group_rows + begin - REACH + lax.broadcasted_iota(jnp.int32, (span, lanes), 0)
-        )
-        outside = (key_pos < 0) | (key_pos >= total_rows)
-        band = lax.dot_general(kv[around, 0:HEAD_DIM], q, contract, preferred_element_type=F32)
-        band = jnp.where(outside, MASKED_SCORE, band * factor + bias[...])
+            sp * group_rows + begin - REACH + lax.broadcasted_iota(jnp.int32, (span, LANES), 0)
+        )
+        edge[...] = jnp.where((key_pos < 0) | (key_pos >= total_rows), MASKED_SCORE, 0.0)
         ctx_keys = ctx_kv[:, :, 0:HEAD_DIM].reshape(ctx_total, HEAD_DIM)
         ctx_values = ctx_kv[:, :, HEAD_DIM:].reshape(ctx_total, HEAD_DIM)
-        far_logits = lax.dot_general(ctx_keys, q, contract, preferred_element_type=F32) * factor
+        band_keys, band_values = kv[around, 0:HEAD_DIM], kv[around, HEAD_DIM:]
         sinks = jnp.concatenate(
             [jnp.broadcast_to(sink[0:1, i : i + 1] * LOG2E, (1, both)) for i in range(2)], axis=1
         )
-        top = jnp.maximum(
-            jnp.maximum(
-                jnp.max(band, axis=0, keepdims=True), jnp.max(far_logits, axis=0, keepdims=True)
-            ),
-            sinks,
-        )
-        band_exp = jnp.exp2(band - top)
-        far_exp = jnp.exp2(far_logits - top)
-        total = (
-            jnp.sum(band_exp, axis=0, keepdims=True)
-            + jnp.sum(far_exp, axis=0, keepdims=True)
-            + jnp.exp2(sinks - top)
-        )
-        mixed = lax.dot_general(
-            kv[around, HEAD_DIM:], band_exp.astype(BF16), across, preferred_element_type=F32
-        ) + lax.dot_general(
-            ctx_values, far_exp.astype(BF16), across, preferred_element_type=F32
-        )
-        mixed = (mixed / total).T.astype(BF16)
+        groups = [slice(0, 2 * LANES), slice(2 * LANES, lanes)]
+        logits = []
+        for g in groups:
+            logits.append(
+                (
+                    lax.dot_general(band_keys, q[g], contract, preferred_element_type=F32),
+                    lax.dot_general(ctx_keys, q[g], contract, preferred_element_type=F32),
+                )
+            )
+        mixed = []
+        for g, (band, far_logits) in zip(groups, logits):
+            wide = (g.stop - g.start) // LANES
+            band = band * factor + bias[:, g] + jnp.concatenate([edge[...]] * wide, axis=1)
+            far_logits = far_logits * factor
+            top = jnp.maximum(
+                jnp.maximum(
+                    jnp.max(band, axis=0, keepdims=True),
+                    jnp.max(far_logits, axis=0, keepdims=True),
+                ),
+                sinks[:, g],
+            )
+            band_exp = jnp.exp2(band - top)
+            far_exp = jnp.exp2(far_logits - top)
+            total = (
+                jnp.sum(band_exp, axis=0, keepdims=True)
+                + jnp.sum(far_exp, axis=0, keepdims=True)
+                + jnp.exp2(sinks[:, g] - top)
+            )
+            summed = lax.dot_general(
+                band_values, band_exp.astype(BF16), across, preferred_element_type=F32
+            ) + lax.dot_general(
+                ctx_values, far_exp.astype(BF16), across, preferred_element_type=F32
+            )
+            mixed.append((summed / total).T.astype(BF16))
+        mixed = jnp.concatenate(mixed, axis=0)
         for h in range(2):
             att[:, h * HEAD_DIM : (h + 1) * HEAD_DIM] = mixed[h * both : (h + 1) * both]
 
@@ -558,36 +587,31 @@
     def give_copy(k):
         return rcopy(give.at[k], pin.at[k], give_send.at[0], give_recv.at[k], tp=partner)
 
-    def relay_copy(up):
-        part, i, to = (low, 0, xp) if up else (high, 1, xm)
-        return rcopy(outx.at[0, part], relay_in.at[i], rel_send.at[0], rel_recv.at[i], tp=to)
-
-    def x_copy(i):
-        part = high if i in (0, 3) else low
-        side = i // 2
+    def x_copy(side):
         return rcopy(
-            outx.at[1 + side, part],
-            x_in.at[side, part],
+            outx.at[side],
+            x_in.at[side],
             xs_send.at[0],
             xs_recv.at[0],
             tp=xm if side else xp,
         )
 
-    n_tile = width
-
-    def project(k):
-        for first, store in ((0, "give"), (rows, "keep")):
-            for j in range(width // n_tile):
-                cols = slice(j * n_tile, (j + 1) * n_tile)
-                value = jnp.dot(
-                    att[first : first + rows, :], wo[:, cols], preferred_element_type=F32
+    def att_copy():
+        return rcopy(att_out, att_in, att_send.at[0], att_recv.at[0], tp=far)
+
+    n_tile = 512
+
+    def project(k, with_far):
+        for j in range(width // n_tile):
+            cols = slice(j * n_tile, (j + 1) * n_tile)
+            value = jnp.dot(att[...], wo[:, cols], preferred_element_type=F32)
+            if with_far:
+                value = value + jnp.dot(
+                    att_in[...], wo_far[:, cols], preferred_element_type=F32
                 )
-                if store == "give":
-                    give[k, :, cols] = value.astype(BF16)
-                else:
-                    kept[:, cols] = value
-            if store == "give":
-                give_copy(k).start()
+            give[k, :, cols] = value[0:rows].astype(BF16)
+            kept[:, cols] = value[rows:]
+        give_copy(k).start()
 
     def add_given(k, store):
         give_copy(k).wait_recv()
@@ -601,17 +625,17 @@
     def chip_block(k):
         attend(chip_of(k))
 
-        @pl.when(k > 0)
+        @pl.when(k == 0)
+        def _():
+            att_out[...] = att[...]
+            att_copy().start()
+
+        @pl.when(k >= 2)
         def _():
             def store(at, value):
-                outx[k - 1, at, :] = value.astype(BF16)
-
-            add_given(k - 1, store)
-
-        @pl.when(k == 1)
-        def _():
-            relay_copy(True).start()
-            relay_copy(False).start()
+                outx[k - 2, at, :] = value.astype(BF16)
+
+            add_given(k - 2, store)
 
         @pl.when(k == 2)
         def _():
@@ -619,29 +643,22 @@
 
         @pl.when(k == 3)
         def _():
-            x_copy(2).start()
-
-        project(k)
+            x_copy(1).start()
+
+        @pl.when((k == 1) | (k == 2))
+        def _():
+            project(k - 1, False)
+
 
     loop(0, NX, chip_block)
 
-    for up, i in ((True, 1), (False, 3)):
-        part, side = (low, 0) if up else (high, 1)
-        relay_copy(up).wait_recv()
-        for s in range(half // 16):
-            at = pl.ds((0 if up else half) + 16 * s, 16)
-            outx[1 + side, at, :] = (
-                outx[1 + side, at, :].astype(F32)
-                + relay_in[side, pl.ds(16 * s, 16), :].astype(F32)
-            ).astype(BF16)
-        x_copy(i).start()
-
-    def own_store(at, value):
-        kept[at, :] = value
-
-    add_given(NX - 1, own_store)
-    z_sent = z_in.at[pl.ds(0, 7)]
-    rcopy(z_sent, z_sent, z_send.at[0], z_recv.at[0], sp=sp).wait_send()
+    att_copy().wait_recv()
+    shared = wo_far.at[pl.ds(0, (NY - 1) * wo_part)]
+    for sem in (2, 3):
+        rcopy(shared, shared, wf_send.at[0], wf_recv.at[sem], sp=sp).wait_recv()
+    project(2, True)
+
+    z_total.wait_send()
     xy_total.wait_send()
     sent = lat.at[pl.ds(0, 7)]
     rcopy(sent, sent, lat_send.at[0], lat_recv.at[0, 0], sp=sp).wait_send()
@@ -659,6 +676,10 @@
     def whole_copy(ref, ssem, rsem):
         return rcopy(ref, ref, ssem, rsem, sp=sp)
 
+    def own_store(at, value):
+        kept[at, :] = value
+
+    add_given(2, own_store)
     whole_copy(x_in, xs_send.at[0], xs_recv.at[0]).wait_recv()
 
     def finish(i):
@@ -669,8 +690,9 @@
     loop(0, rows // strip, finish)
 
     whole_copy(give, give_send.at[0], give_recv.at[0]).wait_send()
-    whole_copy(outx.at[0], rel_send.at[0], rel_recv.at[0]).wait_send()
-    whole_copy(outx.at[pl.ds(1, 2)], xs_send.at[0], xs_recv.at[0]).wait_send()
+    whole_copy(outx, xs_send.at[0], xs_recv.at[0]).wait_send()
+    whole_copy(wo_far, wf_send.at[0], wf_recv.at[0]).wait_send()
+    att_copy().wait_send()
 
 
 def angle_tables(total_rows, n_sp):
@@ -727,8 +749,6 @@
     dma = pltpu.SemaphoreType.DMA
     vmem = pl.BlockSpec(memory_space=pltpu.VMEM)
     anywhere = pl.BlockSpec(memory_space=pltpu.HBM)
-    half = rows // 2
-
     def like(array):
         return pltpu.VMEM(array.shape, array.dtype)
 
@@ -758,7 +778,7 @@
             pltpu.VMEM((width, 2 * HEAD_DIM), BF16),
             like(out_weight),
             pltpu.VMEM((n_tp, rows, width), BF16),
-            pltpu.VMEM((10, groups, 1, LANES), F32),
+            pltpu.VMEM((n_z, groups, 1, LANES), F32),
             pltpu.VMEM((NY * n_tp, groups, 1, LANES), F32),
             pltpu.VMEM((n_tp, rows, LANES), F32),
             pltpu.VMEM((8, width), F32),
@@ -768,16 +788,19 @@
             pltpu.VMEM((group_rows + 2 * REACH, 2 * HEAD_DIM), BF16),
             pltpu.VMEM((n_sp, ctx_rows, 2 * HEAD_DIM), BF16),
             pltpu.VMEM((2 * rows, query_width), BF16),
-            pltpu.VMEM((4, rows, width), BF16),
-            pltpu.VMEM((4, rows, width), BF16),
             pltpu.VMEM((3, rows, width), BF16),
-            pltpu.VMEM((2, half, width), BF16),
+            pltpu.VMEM((3, rows, width), BF16),
             pltpu.VMEM((2, rows, width), BF16),
+            pltpu.VMEM((2, rows, width), BF16),
+            pltpu.VMEM((2 * rows, query_width), BF16),
+            pltpu.VMEM((2 * rows, query_width), BF16),
+            like(out_weight),
             pltpu.VMEM((rows, width), F32),
             pltpu.VMEM((2 * rows + 2 * REACH, 4 * rows), F32),
+            pltpu.VMEM((2 * rows + 2 * REACH, LANES), F32),
             dma((15,)),
             dma((1,)),
-            dma((3,)),
+            dma((1,)),
             dma((1,)),
             dma((1,)),
             dma((1,)),
@@ -787,11 +810,13 @@
             dma((2,)),
             dma((2,)),
             dma((1,)),
+            dma((3,)),
+            dma((1,)),
+            dma((1,)),
+            dma((1,)),
+            dma((1,)),
+            dma((1,)),
             dma((4,)),
-            dma((1,)),
-            dma((2,)),
-            dma((1,)),
-            dma((1,)),
         ],
         compiler_params=pltpu.CompilerParams(
             collective_id=0, has_side_effects=True, vmem_limit_bytes=int(60 * 1024 * 1024)

time: 67.2 us -> 65.2 us (0.970); the launches traced: 67.1 us -> 64.1 us
  Pallas kernels: 66.3 us -> 63.3 us
    pallas_call x1, Pallas kernels: 66.3 us -> 63.3 us  [shards(): pl.pallas_call(functools.partial(block_kernel, n_sp, n_tp), out_shape=plt...]
where the time goes in v3:
time: 65.2 us; the launch traced here: 64.1 us
  Pallas kernels  63.3 us (97%)
  local copies, waits for them, and re-layouts  0.75 us (1%)
    pallas_call x1, Pallas kernels, shards(): pl.pallas_call(functools.partial(block_kernel, n_sp, n_tp), out_shape=plt...  63.3 us

profile of v3, /device:TPU:1, one launch (start us, length us, event | category | flops | bytes accessed | tf_op | source)
XLA Modules:
  0.0 64.1 jit_solution(10810894760774717169)
XLA Ops:
  0.0 63.3 %shard_map.145 = bf16[96,2048]{1,0:T(8,128)(2,1)S(1)} custom-call(f32[1,32]{1,0:T(1,128)} %bitcast.5, f32[1,32]{1,0:T(1,128)} %bitcast.6, f32[1,2048]{1,0:T(1,128)} %bitcast.4, f32[1,2]{1,0:T(1,128)} %bitcast.7, f32[64,32,128]{2,1,0:T(8,128)} %constant.4.clone.rot_row_hbm, f32[128,128]{1,0:T(8,128)} %constant.5.clone.rot_col_hbm, ...), custom_call_target="tpu_custom_call" | custom-call | tf_op jit(solution)/shard_map/pallas_call | solution.py:759
  63.3 0.7 %copy.17 = bf16[96,2048]{1,0:T(8,128)(2,1)} copy(bf16[96,2048]{1,0:T(8,128)(2,1)S(1)} %shard_map.145) | data formatting | bytes 786432

commit v4 on v3

--- a/solution.py
+++ b/solution.py
@@ -371,7 +371,7 @@
     def ctx_z(i):
         return ctx_copy(sp, zs[near_first(i)] * NY + y, z)
 
-    for i in range(n_z - 1):
+    for i in (14, 13, 12, 0, 1, 11, 10, 2, 3, 9, 8, 4, 5, 7, 6):
         ctx_z(i).start()
 
     relay_a = lat_copy(xm, low, 6, xp)
@@ -587,15 +587,6 @@
     def give_copy(k):
         return rcopy(give.at[k], pin.at[k], give_send.at[0], give_recv.at[k], tp=partner)
 
-    def x_copy(side):
-        return rcopy(
-            outx.at[side],
-            x_in.at[side],
-            xs_send.at[0],
-            xs_recv.at[0],
-            tp=xm if side else xp,
-        )
-
     def att_copy():
         return rcopy(att_out, att_in, att_send.at[0], att_recv.at[0], tp=far)
 
@@ -616,11 +607,9 @@
     def add_given(k, store):
         give_copy(k).wait_recv()
 
-        def one(i):
-            at = pl.ds(pl.multiple_of(i * strip, strip), strip)
+        for i in range(rows // strip):
+            at = pl.ds(i * strip, strip)
             store(at, kept[at, :] + pin[k, at, :].astype(F32))
-
-        loop(0, rows // strip, one)
 
     def chip_block(k):
         attend(chip_of(k))
@@ -630,20 +619,21 @@
             att_out[...] = att[...]
             att_copy().start()
 
-        @pl.when(k >= 2)
-        def _():
-            def store(at, value):
-                outx[k - 2, at, :] = value.astype(BF16)
-
-            add_given(k - 2, store)
-
-        @pl.when(k == 2)
-        def _():
-            x_copy(0).start()
-
-        @pl.when(k == 3)
-        def _():
-            x_copy(1).start()
+        for side in range(2):
+
+            @pl.when(k == 2 + side)
+            def _():
+                def store(at, value):
+                    outx[side, at, :] = value.astype(BF16)
+                    rcopy(
+                        outx.at[side, at],
+                        x_in.at[side, at],
+                        xs_send.at[0],
+                        xs_recv.at[0],
+                        tp=xm if side else xp,
+                    ).start()
+
+                add_given(side, store)
 
         @pl.when((k == 1) | (k == 2))
         def _():

time: 65.2 us -> 63 us (0.966)
  Pallas kernels: 63.3 us -> 61.8 us
    pallas_call x1, Pallas kernels: 63.3 us -> 61.8 us  [shards(): pl.pallas_call(functools.partial(block_kernel, n_sp, n_tp), out_shape=plt...]
where the time goes in v4:
time: 63 us; the launch traced here: 62.5 us
  Pallas kernels  61.8 us (98%)
  local copies, waits for them, and re-layouts  0.75 us (1%)
    pallas_call x1, Pallas kernels, shards(): pl.pallas_call(functools.partial(block_kernel, n_sp, n_tp), out_shape=plt...  61.8 us

profile of v4, /device:TPU:1, one launch (start us, length us, event | category | flops | bytes accessed | tf_op | source)
XLA Modules:
  0.0 62.5 jit_solution(11419114799457223554)
XLA Ops:
  0.0 61.8 %shard_map.145 = bf16[96,2048]{1,0:T(8,128)(2,1)S(1)} custom-call(f32[1,32]{1,0:T(1,128)} %bitcast.5, f32[1,32]{1,0:T(1,128)} %bitcast.6, f32[1,2048]{1,0:T(1,128)} %bitcast.4, f32[1,2]{1,0:T(1,128)} %bitcast.7, f32[64,32,128]{2,1,0:T(8,128)} %constant.4.clone.rot_row_hbm, f32[128,128]{1,0:T(8,128)} %constant.5.clone.rot_col_hbm, ...), custom_call_target="tpu_custom_call" | custom-call | tf_op jit(solution)/shard_map/pallas_call | solution.py:749
  61.8 0.7 %copy.17 = bf16[96,2048]{1,0:T(8,128)(2,1)} copy(bf16[96,2048]{1,0:T(8,128)(2,1)S(1)} %shard_map.145) | data formatting | bytes 786432

commit v5 on v4

--- a/solution.py
+++ b/solution.py
@@ -315,14 +315,14 @@
             tp=to_tp,
         )
 
-    for d in range(1, NY * n_tp):
-        xy_copy(d, True).start()
+    for dy in (2, 1, 3, 0):
+        for dt in (4, 3, 5, 2, 6, 1, 7, 0):
+            if dy or dt:
+                xy_copy(dy * n_tp + dt, True).start()
 
     for part, i, to in ((high, 2, xp), (low, 3, xm)):
         copy = lat_copy(tp, part, i, to)
         copy.start()
-
-    far_weights(wo, sp, far, 1, 1).start()
 
     for i, slot, order in ((0, xm, (0,)), (1, xp, (1,))):
         for j in order:
@@ -378,6 +378,7 @@
     relay_a.start()
     relay_b = lat_copy(xp, high, 7, xm)
     relay_b.start()
+    far_weights(wo, sp, far, 1, 1).start()
 
     def ctx_y(i, d):
         slot = (zs[near_first(i - 1)] if i else z) * NY + y

time: 63 us -> 62.3 us (0.989)
  Pallas kernels: 61.8 us -> 61.1 us
    pallas_call x1, Pallas kernels: 61.8 us -> 61.1 us  [shards(): pl.pallas_call(functools.partial(block_kernel, n_sp, n_tp), out_shape=plt...]
where the time goes in v5:
time: 62.3 us; the launch traced here: 61.8 us
  Pallas kernels  61.1 us (98%)
  local copies, waits for them, and re-layouts  0.75 us (1%)
    pallas_call x1, Pallas kernels, shards(): pl.pallas_call(functools.partial(block_kernel, n_sp, n_tp), out_shape=plt...  61.1 us

profile of v5, /device:TPU:1, one launch (start us, length us, event | category | flops | bytes accessed | tf_op | source)
XLA Modules:
  0.0 61.8 jit_solution(4361236498576999055)
XLA Ops:
  0.0 61.1 %shard_map.145 = bf16[96,2048]{1,0:T(8,128)(2,1)S(1)} custom-call(f32[1,32]{1,0:T(1,128)} %bitcast.5, f32[1,32]{1,0:T(1,128)} %bitcast.6, f32[1,2048]{1,0:T(1,128)} %bitcast.4, f32[1,2]{1,0:T(1,128)} %bitcast.7, f32[64,32,128]{2,1,0:T(8,128)} %constant.4.clone.rot_row_hbm, f32[128,128]{1,0:T(8,128)} %constant.5.clone.rot_col_hbm, ...), custom_call_target="tpu_custom_call" | custom-call | tf_op jit(solution)/shard_map/pallas_call | solution.py:750
  61.1 0.7 %copy.17 = bf16[96,2048]{1,0:T(8,128)(2,1)} copy(bf16[96,2048]{1,0:T(8,128)(2,1)S(1)} %shard_map.145) | data formatting | bytes 786432
